TPU v7x, 128 devices: a whole 4x4x4 slice. The times are simulated.
128 devices in a mesh: sp: 32 (over z, y, core), tp: 4 (over x).
Axes of the slice: x: 4, y: 4, z: 4, core: 2. Of those that a mesh axis runs over, the one named last changes fastest.
Arguments:
- query_narrow: bfloat16 [4096, 2048], P('sp', 'tp'), may hold values from -48 to 48
- key_narrow: bfloat16 [4096, 512], P('sp', 'tp'), may hold values from -15 to 15
- value_narrow: bfloat16 [4096, 512], P('sp', 'tp'), may hold values from -6 to 6
- gates_narrow: float32 [4096, 16], P(None, 'tp'), may hold values from -514 to 0, as said below
- query_broad: bfloat16 [4096, 2048], P('sp', 'tp'), may hold values from -48 to 48
- key_broad: bfloat16 [4096, 1024], P('sp', 'tp'), may hold values from -15 to 15
- value_broad: bfloat16 [4096, 1024], P('sp', 'tp'), may hold values from -6 to 6
- gates_broad: float32 [4096, 8], P(None, 'tp'), may hold values from -514 to 0, as said below
- project_narrow: bfloat16 [2048, 4096], P('tp'), may hold values from -0.1875 to 0.1875
- project_broad: bfloat16 [2048, 4096], P('tp'), may hold values from -0.1875 to 0.1875
- residual: bfloat16 [4096, 4096], P('sp'), may hold values from -6 to 6
- norm_gain: float32 [4096], replicated, may hold values from 0.1 to 1.9
- route_ids: int32 [4096, 4], P(('sp', 'tp')), may hold values from 0 to 127, all different within a row; in each aligned block of 32 rows (0 to 31, 32 to 63, ...) at most 2 rows name the same one
- route_weight: float32 [4096, 4], P(('sp', 'tp')), may hold values from 0.2 to 1.2
- expert_gate: bfloat16 [128, 4096, 256], P(('sp', 'tp')), may hold values from -0.09375 to 0.09375
- expert_up: bfloat16 [128, 4096, 256], P(('sp', 'tp')), may hold values from -0.09375 to 0.09375
- expert_down: bfloat16 [128, 256, 4096], P(('sp', 'tp')), may hold values from -0.375 to 0.375
- shared_gate: bfloat16 [4096, 1024], P(None, 'tp'), may hold values from -0.09375 to 0.09375
- shared_up: bfloat16 [4096, 1024], P(None, 'tp'), may hold values from -0.09375 to 0.09375
- shared_down: bfloat16 [1024, 4096], P('tp'), may hold values from -0.1875 to 0.1875
Outputs:
- layer_out: bfloat16 [4096, 4096], P(('sp', 'tp'))
Inputs may be any that keep to these rules, and one draw needn't show every extreme that they name: `gates_narrow`: Non-increasing along positions in each head. `gates_broad`: Non-increasing along positions in each head. `route_ids`: each row names 4 different experts; among the rows of one device no expert is named by more than 2 rows, and that number is reached.
All inputs are finite; a program needn't handle non-finite values.
Results may differ from a plain program's by a relative error of at most 0.014.
Values may be sent and summed in bfloat16 or wider, within the bound.
A program may use at most 128 MiB of HBM per device.

v0:
```python
import math

import jax
import jax.numpy as jnp
from jax import lax
from jax.sharding import PartitionSpec as P

NARROW_SIZE = 128
BROAD_SIZE = 256


norm_epsilon = 1e-06


def in_one_piece(arrays, axis, dim, along):
    both = jnp.concatenate(arrays, axis=along)
    whole, at, outs = (lax.all_gather(both, axis, axis=dim, tiled=True), 0, [])
    for a in arrays:
        outs.append(lax.slice_in_dim(whole, at, at + a.shape[along], axis=along))
        at += a.shape[along]
    return tuple(outs)


def split_up(shard, dim, length):
    dims = shard.shape
    parts = shard.reshape(*dims[:dim], length, dims[dim] // length, *dims[dim + 1 :])
    return jnp.moveaxis(parts, dim, 0)


def sum_at_owner(shard, axis, dim):
    length = lax.axis_size(axis)
    parts = lax.all_to_all(split_up(shard, dim, length), axis, 0, 0, tiled=True)
    return jnp.sum(parts.astype(jnp.float32), axis=0)


def span_for(length):
    common = math.gcd(length, 512)
    return common


def split_heads(rows, kv_local, head_size):
    tokens = rows.shape[0]
    group_size = rows.shape[1] // (kv_local * head_size)
    return rows.reshape(tokens, kv_local, group_size, head_size).transpose(1, 2, 0, 3)


def attend_span(
    states,
    queries,
    query_gates,
    key_rows,
    value_rows,
    key_gates,
    query_place,
    key_place,
    key_limit,
    scaling,
):
    kv_local, group_size, tokens, head_size = queries.shape
    length = key_rows.shape[0]
    key_heads = key_rows.reshape(length, kv_local, head_size)
    value_heads = value_rows.reshape(length, kv_local, head_size)
    scores = (
        jnp.einsum("kgtd,skd->kgts", queries, key_heads, preferred_element_type=jnp.float32)
        * scaling
    )
    scores = scores + query_gates[..., None] - key_gates.T.reshape(kv_local, group_size, 1, length)
    allowed = (key_place[None, :] <= query_place[:, None]) & (key_place[None, :] < key_limit)
    scores = jnp.where(allowed, scores, -jnp.inf)
    running_max, running_sum, weighted = states
    newest = jnp.maximum(running_max, jnp.max(scores, axis=-1))
    anchor = jnp.where(newest == -jnp.inf, 0.0, newest)
    weights = jnp.exp(scores - anchor[..., None])
    factor = jnp.exp(running_max - anchor)
    weighted = weighted * factor[..., None] + jnp.einsum(
        "kgts,skd->kgtd",
        weights.astype(jnp.bfloat16),
        value_heads,
        preferred_element_type=jnp.float32,
    )
    running_sum = running_sum * factor + jnp.sum(weights, axis=-1)
    return (newest, running_sum, weighted)


def local(
    query_narrow,
    key_narrow,
    value_narrow,
    gates_narrow,
    query_broad,
    key_broad,
    value_broad,
    gates_broad,
    project_narrow,
    project_broad,
    residual,
    norm_gain,
    route_ids,
    route_weight,
    expert_gate,
    expert_up,
    expert_down,
    shared_gate,
    shared_up,
    shared_down,
):
    tokens = query_narrow.shape[0]
    first_row = lax.axis_index("sp") * tokens
    query_place = first_row + jnp.arange(tokens, dtype=jnp.int32)
    groups_info = []
    for queries, all_gates, head_size, key_width in (
        (query_narrow, gates_narrow, NARROW_SIZE, key_narrow.shape[1]),
        (query_broad, gates_broad, BROAD_SIZE, key_broad.shape[1]),
    ):
        kv_local = key_width // head_size
        split = split_heads(queries, kv_local, head_size)
        own_gates = lax.dynamic_slice_in_dim(all_gates, first_row, tokens, 0)
        own_gates = own_gates.reshape(tokens, kv_local, -1).transpose(1, 2, 0)
        groups_info.append((split, own_gates, all_gates, head_size ** (-0.5)))

    def update(states, pairs, key_first, key_limit):
        length = pairs[0][0].shape[0]
        key_place = key_first + jnp.arange(length, dtype=jnp.int32)
        result = []
        for details, member, key_value in zip(groups_info, states, pairs):
            split, own_gates, all_gates, scaling = details
            key_gates = lax.dynamic_slice_in_dim(all_gates, key_first, length, 0)
            result.append(
                attend_span(
                    member,
                    split,
                    own_gates,
                    key_value[0],
                    key_value[1],
                    key_gates,
                    query_place,
                    key_place,
                    key_limit,
                    scaling,
                )
            )
        return tuple(result)

    empty = tuple(
        (
            (
                jnp.full(details[0].shape[:3], -jnp.inf, jnp.float32),
                jnp.zeros(details[0].shape[:3], jnp.float32),
                jnp.zeros(details[0].shape, jnp.float32),
            )
            for details in groups_info
        )
    )
    key_limit = first_row + tokens
    narrow_keys, narrow_values, broad_keys, broad_values = in_one_piece(
        (key_narrow, value_narrow, key_broad, value_broad), "sp", 0, 1
    )
    length = narrow_keys.shape[0]
    stride = span_for(length)

    def one_span(round_index, carried):
        offset = round_index * stride

        def cut(array):
            return lax.dynamic_slice_in_dim(array, offset, stride, 0)

        def take(inner):
            return update(
                inner,
                ((cut(narrow_keys), cut(narrow_values)), (cut(broad_keys), cut(broad_values))),
                offset,
                key_limit,
            )

        def leave(inner):
            return inner

        return lax.cond(offset < key_limit, take, leave, carried)

    finished = lax.fori_loop(0, length // stride, one_span, empty)
    heads_out = []
    for running_max, running_sum, weighted in finished:
        normalized = (weighted / running_sum[..., None]).astype(jnp.bfloat16)
        heads_out.append(normalized.transpose(2, 0, 1, 3).reshape(tokens, -1))
    partial_value = jnp.dot(heads_out[0], project_narrow, preferred_element_type=jnp.float32)
    partial_value = partial_value + jnp.dot(
        heads_out[1], project_broad, preferred_element_type=jnp.float32
    )
    mixture = lax.psum(partial_value.astype(jnp.bfloat16), "tp").astype(jnp.float32)
    stream = residual.astype(jnp.float32) + mixture
    normed = (
        stream
        * lax.rsqrt(jnp.mean(stream * stream, axis=-1, keepdims=True) + norm_epsilon)
        * norm_gain
    ).astype(jnp.bfloat16)
    shared_hidden = (
        jax.nn.silu(jnp.dot(normed, shared_gate, preferred_element_type=jnp.float32))
        * jnp.dot(normed, shared_up, preferred_element_type=jnp.float32)
    ).astype(jnp.bfloat16)
    sub_rows = route_ids.shape[0]
    own_first = lax.axis_index("tp") * sub_rows
    shared = sum_at_owner(
        jnp.dot(shared_hidden, shared_down, preferred_element_type=jnp.float32).astype(
            jnp.bfloat16
        ),
        "tp",
        0,
    )
    top_count = route_ids.shape[1]
    local_experts = expert_gate.shape[0]
    expert_total = lax.axis_size("sp") * lax.axis_size("tp") * local_experts
    capacity = 2 * sub_rows * top_count // expert_total
    flat_ids = route_ids.reshape(-1)
    one_hot = (flat_ids[:, None] == jnp.arange(expert_total, dtype=jnp.int32)[None, :]).astype(
        jnp.int32
    )
    slot_of = jnp.sum(one_hot * (jnp.cumsum(one_hot, axis=0) - 1), axis=1)
    target = (flat_ids * capacity + slot_of).reshape(sub_rows, top_count)
    slot_total = expert_total * capacity
    matches = target[None, :, :] == jnp.arange(slot_total, dtype=jnp.int32)[:, None, None]
    dispatch = jnp.any(matches, axis=-1).astype(jnp.bfloat16)
    own_normed = lax.dynamic_slice_in_dim(normed, own_first, sub_rows, 0)
    outbound = (
        jnp.dot(dispatch, own_normed, preferred_element_type=jnp.float32)
        .astype(jnp.bfloat16)
        .reshape(expert_total, capacity, -1)
    )
    weight_rounded = route_weight.astype(jnp.bfloat16)
    combiner = jnp.sum(
        jnp.where(matches, weight_rounded[None], jnp.zeros((), jnp.bfloat16)), axis=-1
    ).T
    inbound = lax.all_to_all(outbound, ("sp", "tp"), split_axis=0, concat_axis=0, tiled=True)
    senders = inbound.shape[0] // local_experts
    grouped = inbound.reshape(senders, local_experts, inbound.shape[1], inbound.shape[2])
    gate_out = jnp.einsum(
        "secd,edh->sech", grouped, expert_gate, preferred_element_type=jnp.float32
    )
    up_out = jnp.einsum("secd,edh->sech", grouped, expert_up, preferred_element_type=jnp.float32)
    hidden = (jax.nn.silu(gate_out) * up_out).astype(jnp.bfloat16)
    result = jnp.einsum(
        "sech,ehd->secd", hidden, expert_down, preferred_element_type=jnp.float32
    ).astype(jnp.bfloat16)
    results = result.reshape(inbound.shape)
    returned = lax.all_to_all(results, ("sp", "tp"), split_axis=0, concat_axis=0, tiled=True)
    routed = jnp.dot(combiner, returned.reshape(slot_total, -1), preferred_element_type=jnp.float32)
    own_stream = lax.dynamic_slice_in_dim(stream, own_first, sub_rows, 0)
    return (own_stream + shared + routed).astype(jnp.bfloat16)


def solution(mesh):
    placed = (
        P("sp", "tp"),
        P("sp", "tp"),
        P("sp", "tp"),
        P(None, "tp"),
        P("sp", "tp"),
        P("sp", "tp"),
        P("sp", "tp"),
        P(None, "tp"),
        P("tp", None),
        P("tp", None),
        P("sp", None),
        P(),
        P(("sp", "tp"), None),
        P(("sp", "tp"), None),
        P(("sp", "tp"), None, None),
        P(("sp", "tp"), None, None),
        P(("sp", "tp"), None, None),
        P(None, "tp"),
        P(None, "tp"),
        P("tp", None),
    )
    return jax.shard_map(
        local, mesh=mesh, in_specs=placed, out_specs=P(("sp", "tp"), None), check_vma=False
    )
```

profile of v0, /device:TPU:1, one launch (start us, length us, event | category | flops | bytes accessed | tf_op | source)
XLA Modules:
  0.0 299.0 jit_solution(1453185535958948922)
XLA Ops:
  6.5 1.7 pad_maximum_fusion
  8.3 1.0 copy.74
  9.4 0.1 copy.76
  9.5 1.0 copy.75
  10.5 0.1 copy.77
  10.7 0.7 dynamic-slice_bitcast_fusion.3
  11.4 0.7 dynamic-slice_bitcast_fusion.2
  12.0 50.3 %all-gather.2.cloned.1.call-done = bf16[4096,768]{1,0:T(8,128)(2,1)} async-done(((bf16[128,768]{1,0:T(8,128)(2,1)}), bf16[4096,768]{1,0:T(8,128)(2,1)}) %all-gather.2.cloned.1.call-update) | async-done | bytes 6291472 | tf_op jit(solution)/shard_map/all_gather | solution.py:17
  62.4 4.5 %fusion.99 = (bf16[4096,256]{1,0:T(8,128)(2,1)}, bf16[4096,256]{1,0:T(8,128)(2,1)}) fusion(bf16[4096,768]{1,0:T(8,128)(2,1)} %all-gather.2.cloned.1.call-done), kind=kLoop, calls=%fused_computation.112 | loop fusion | bytes 8388608 | tf_op jit(solution)/shard_map/slice | solution.py:19
  66.9 3.0 fusion.100
  70.0 7.7 %while.24 = (s32[]{:T(128)}, f32[1,4,128]{2,1,0:T(4,128)S(1)}, f32[1,4,128]{2,1,0:T(4,128)S(1)}, f32[1,4,128,128]{3,2,1,0:T(8,128)S(1)}, f32[1,2,128]{2,1,0:T(2,...) while((s32[]{:T(128)}, f32[1,4,128]{2,1,0:T(4,128)S(1)}, ...), condition=%wide.region_7.8_spmd.clone, body=%wide.region_0.7_spmd.clone.sunk | while | flops 272376192 | bytes 7115305 | solution.py:180
  70.0 7.2 %conditional.3 = ((f32[1,4,128]{2,1,0:T(4,128)S(1)}, f32[1,4,128]{2,1,0:T(4,128)S(1)}, f32[1,4,128,128]{3,2,1,0:T(8,128)S(1)}, f32[1,2,128]{2,1,0:T(2,128)S(1)},...) conditional(s32[]{:T(128)} %convert_element_type.115, (f32[1,4,128]{2,1,0:T(4,128)S(1)}, ...), branch_computations={%region_1.0_spmd, %region_2.6_spmd} | conditional | flops 272376192 | bytes 7114370 | solution.py:178
  70.1 0.7 dynamic-slice_bitcast_fusion.1
  70.8 0.2 compare_and_fusion
  71.0 1.3 fusion.98
  72.3 1.3 fusion.11
  73.7 0.7 dynamic-slice_bitcast_fusion
  74.4 1.3 fusion.97
  75.7 1.3 fusion.10
  77.0 0.2 fusion.13
  77.7 0.1 copy.79
  77.8 0.1 copy.78
  78.0 3.1 %fusion.101 = f32[128,4096]{1,0:T(8,128)S(1)} fusion(bf16[128,512]{0,1:T(8,128)(2,1)S(1)} %bitcast.155, bf16[512,4096]{1,0:T(8,128)(2,1)} %param.32), kind=kOutput, calls=%fused_computation.114 | convolution fusion | flops 536870912 | bytes 6422528 | tf_op jit(solution)/shard_map/dot_general | solution.py:185
  81.1 0.4 copy-done.1
  81.5 1.7 fusion.38
  83.3 0.1 eq.34
  83.5 0.2 reduce_window_sum.11
  83.7 0.2 select_reduce_fusion
  83.9 0.1 reduce_sum.66
  84.1 0.1 fusion.84
  84.2 92.1 %all-reduce.2.cloned.1.call-done = bf16[128,4096]{1,0:T(8,128)(2,1)} async-done(((bf16[128,4096]{1,0:T(8,128)(2,1)}), bf16[128,4096]{1,0:T(8,128)(2,1)}) %all-reduce.2.cloned.1.call-update) | async-done | bytes 1048592 | tf_op jit(solution)/shard_map/psum | solution.py:189
  176.3 3.1 %convert_add_fusion = (f32[128,4096]{1,0:T(8,128)}, f32[128]{0:T(128)S(1)}) fusion(bf16[128,4096]{1,0:T(8,128)(2,1)} %all-reduce.2.cloned.1.call-done, bf16[128,4096]{1,0:T(8,128)(2,1)S(1)} %copy-done.2), kind=kLoop, calls=%fused_computation.70 | loop fusion | flops 2621312 | bytes 4194816 | tf_op jit(solution)/shard_map/add | solution.py:190
  179.4 0.5 multiply_convert_fusion
  179.8 2.0 convolution_convert_fusion.1
  181.9 4.4 %reshape.159 = bf16[128,2,4096]{2,1,0:T(2,128)(2,1)} reshape(bf16[256,4096]{1,0:T(8,128)(2,1)} %convolution_convert_fusion.1) | data formatting | bytes 4194304 | tf_op jit(solution)/shard_map/reshape | solution.py:226
  186.3 11.5 %all-to-all-start.1 = ((bf16[128,2,4096]{2,1,0:T(2,128)(2,1)}), bf16[128,2,4096]{2,1,0:T(2,128)(2,1)}, u32[]{:S(2)}, u32[]{:S(2)}) async-start(bf16[128,2,4096]{2,1,0:T(2,128)(2,1)} %reshape.159), calls=%async_computation.1 | async-start | bytes 4194304 | tf_op jit(solution)/shard_map/all_to_all | solution.py:232
  197.8 2.0 fusion.102
  199.8 4.5 %convolution_convert_fusion.2 = bf16[128,4096]{1,0:T(8,128)(2,1)} fusion(bf16[256,4096]{1,0:T(8,128)(2,1)} %param.43, bf16[128,4096]{1,0:T(8,128)(2,1)S(1)} %multiply_convert_fusion, bf16[4096,256]{1,0:T(8,128)(2,1)} %param.42, f32[128,256]{1,0:T(8,128)S(1)} %fusion.102), kind=kOutput, calls=%fused_computation.59 | convolution fusion | flops 537591808 | bytes 6422528 | tf_op jit(solution)/shard_map/dot_general | solution.py:203
  204.4 23.8 %all-to-all-done.1 = bf16[128,2,4096]{2,1,0:T(2,128)(2,1)} async-done(((bf16[128,2,4096]{2,1,0:T(2,128)(2,1)}), bf16[128,2,4096]{2,1,0:T(2,128)(2,1)}, u32[]{:S(2)}, u32[]{:S(2)}) %all-to-all-start.1) | async-done | bytes 2097184 | tf_op jit(solution)/shard_map/all_to_all | solution.py:232
  228.2 3.7 %all-to-all-start = ((bf16[4,32,4096]{2,1,0:T(8,128)(2,1)}), bf16[4,32,4096]{2,1,0:T(8,128)(2,1)S(1)}, u32[]{:S(2)}, u32[]{:S(2)}) async-start(bf16[4,32,4096]{2,1,0:T(8,128)(2,1)} %bitcast.153), calls=%async_computation | async-start | bytes 2097152 | tf_op jit(solution)/shard_map/all_to_all | solution.py:32
  231.9 4.6 %fusion.47 = f32[128,1,2,256]{3,0,2,1:T(8,128)S(1)} fusion(bf16[1,4096,256]{2,1,0:T(8,128)(2,1)} %param.38, bf16[128,2,4096]{2,1,0:T(2,128)(2,1)} %all-to-all-done.1), kind=kOutput, calls=%fused_computation.73 | convolution fusion | flops 536870912 | bytes 4456448 | tf_op jit(solution)/shard_map/secd,edh->sech/dot_general | solution.py:235
  236.5 7.1 %convolution_convert_fusion = bf16[128,2,4096]{2,0,1:T(8,128)(2,1)} fusion(bf16[1,256,4096]{2,1,0:T(8,128)(2,1)S(1)} %copy-done, bf16[1,4096,256]{2,1,0:T(8,128)(2,1)} %param.39, bf16[128,2,4096]{2,1,0:T(2,128)(2,1)} %all-to-all-done.1, f32[128,1,2,256]{3,0,2,1:T(8,128)S(1)} %fusion.47), kind=kOutput, calls=%fused_computation.55 | convolution fusion | flops 1075183616 | bytes 8650752 | tf_op jit(solution)/shard_map/sech,ehd->secd/dot_general | solution.py:240
  243.6 5.1 %copy.84 = bf16[128,2,4096]{2,1,0:T(2,128)(2,1)} copy(bf16[128,2,4096]{2,0,1:T(8,128)(2,1)} %convolution_convert_fusion) | data formatting | bytes 4194304 | tf_op jit(solution)/shard_map/convert_element_type | solution.py:242
  248.7 6.0 %all-to-all-start.2 = ((bf16[128,2,4096]{2,1,0:T(2,128)(2,1)}), bf16[128,2,4096]{2,1,0:T(2,128)(2,1)}, u32[]{:S(2)}, u32[]{:S(2)}) async-start(bf16[128,2,4096]{2,1,0:T(2,128)(2,1)} %copy.84), calls=%async_computation.2 | async-start | bytes 4194304 | tf_op jit(solution)/shard_map/all_to_all | solution.py:244
  254.9 1.0 convert_reduce_fusion
  255.8 29.3 %all-to-all-done.2 = bf16[128,2,4096]{2,1,0:T(2,128)(2,1)} async-done(((bf16[128,2,4096]{2,1,0:T(2,128)(2,1)}), bf16[128,2,4096]{2,1,0:T(2,128)(2,1)}, u32[]{:S(2)}, u32[]{:S(2)}) %all-to-all-start.2) | async-done | bytes 2097184 | tf_op jit(solution)/shard_map/all_to_all | solution.py:244
  285.1 4.1 %reshape.164 = bf16[256,4096]{1,0:T(8,128)(2,1)} reshape(bf16[128,2,4096]{2,1,0:T(2,128)(2,1)} %all-to-all-done.2) | data formatting | bytes 4194304 | tf_op jit(solution)/shard_map/reshape | solution.py:245
  289.3 2.8 fusion.39
  (64 shorter events, 0.9 us)
Async XLA Ops:
  6.5 230.0 %copy-start = (bf16[1,256,4096]{2,1,0:T(8,128)(2,1)S(1)}, bf16[1,256,4096]{2,1,0:T(8,128)(2,1)}, u32[]{:S(2)}) copy-start(bf16[1,256,4096]{2,1,0:T(8,128)(2,1)} %param.40) | copy-start | bytes 6291460
  6.5 55.8 %all-gather.2.cloned.1.call-start = ((), (), s32[]{:S(2)}) async-start(), calls=%async_computation.3 | async-start | bytes 6488064 | tf_op jit(solution)/shard_map/all_gather | solution.py:17
  8.3 168.0 %all-reduce.2.cloned.1.call-start = ((), (), s32[]{:S(2)}) async-start(), calls=%async_computation.4 | async-start | bytes 2097152 | tf_op jit(solution)/shard_map/psum | solution.py:189
  78.0 3.5 %copy-start.1 = (bf16[512,4096]{1,0:T(8,128)(2,1)S(1)}, bf16[512,4096]{1,0:T(8,128)(2,1)}, u32[]{:S(2)}) copy-start(bf16[512,4096]{1,0:T(8,128)(2,1)} %param.33) | copy-start | bytes 12582916
  81.5 1.8 copy-start.7
  83.2 93.1 %copy-start.2 = (bf16[128,4096]{1,0:T(8,128)(2,1)S(1)}, bf16[128,4096]{1,0:T(8,128)(2,1)}, u32[]{:S(2)}) copy-start(bf16[128,4096]{1,0:T(8,128)(2,1)} %param.34) | copy-start | bytes 3145732
  84.2 95.1 %copy-start.6 = (f32[4096]{0:T(1024)S(1)}, f32[4096]{0:T(1024)}, u32[]{:S(2)}) copy-start(f32[4096]{0:T(1024)} %param.35) | copy-start | bytes 49156
  176.3 3.1 %copy-start.3 = (bf16[128,4096]{1,0:T(8,128)(2,1)S(1)}, bf16[128,4096]{1,0:T(8,128)(2,1)}, u32[]{:S(2)}) copy-start(bf16[128,4096]{1,0:T(8,128)(2,1)} %param.34) | copy-start | bytes 3145732
  176.3 3.1 %copy-start.4 = (bf16[128,4096]{1,0:T(8,128)(2,1)S(1)}, bf16[128,4096]{1,0:T(8,128)(2,1)}, u32[]{:S(2)}) copy-start(bf16[128,4096]{1,0:T(8,128)(2,1)} %all-reduce.2.cloned.1.call-done) | copy-start | bytes 3145732
  186.3 41.9 %all-to-all-start.1 = ((bf16[128,2,4096]{2,1,0:T(2,128)(2,1)}), bf16[128,2,4096]{2,1,0:T(2,128)(2,1)}, u32[]{:S(2)}, u32[]{:S(2)}) async-start(bf16[128,2,4096]{2,1,0:T(2,128)(2,1)} %reshape.159), calls=%async_computation.1 | async-start | bytes 4194304 | tf_op jit(solution)/shard_map/all_to_all | solution.py:232
  228.2 20.5 %all-to-all-start = ((bf16[4,32,4096]{2,1,0:T(8,128)(2,1)}), bf16[4,32,4096]{2,1,0:T(8,128)(2,1)S(1)}, u32[]{:S(2)}, u32[]{:S(2)}) async-start(bf16[4,32,4096]{2,1,0:T(8,128)(2,1)} %bitcast.153), calls=%async_computation | async-start | bytes 2097152 | tf_op jit(solution)/shard_map/all_to_all | solution.py:32
  248.7 6.1 %copy-start.8 = (f32[32,4]{0,1:T(4,128)S(1)}, f32[32,4]{0,1:T(4,128)}, u32[]{:S(2)}) copy-start(f32[32,4]{0,1:T(4,128)} %param.37) | copy-start | bytes 1540
  248.7 36.5 %all-to-all-start.2 = ((bf16[128,2,4096]{2,1,0:T(2,128)(2,1)}), bf16[128,2,4096]{2,1,0:T(2,128)(2,1)}, u32[]{:S(2)}, u32[]{:S(2)}) async-start(bf16[128,2,4096]{2,1,0:T(2,128)(2,1)} %copy.84), calls=%async_computation.2 | async-start | bytes 4194304 | tf_op jit(solution)/shard_map/all_to_all | solution.py:244
  255.8 33.4 %copy-start.5 = (f32[32,4096]{1,0:T(8,128)S(1)}, f32[32,4096]{1,0:T(8,128)}, u32[]{:S(2)}) copy-start(f32[32,4096]{1,0:T(8,128)} %convert_reduce_fusion) | copy-start | bytes 1572868
Sparse Core Ops, SparseCore 0:
  9.6 52.7 all-gather.1
  83.4 92.8 all-reduce.1
where the time goes:
time: 301 us; the launch traced here: 299 us
  waiting for transfers between devices  196 us (65%)
  matrix products  33.2 us (11%)
  local copies, waits for them, and re-layouts  27.3 us (9%)
  starting transfers between devices  21.3 us (7%)
  between operations  13.7 us (5%)
  other arithmetic  7.44 us (2%)
    psum x1, waiting for transfers between devices, local(): lax.psum(partial_value.astype(jnp.bfloat16), 'tp').astype(jnp.float32)  92.1 us
    all_gather x1, waiting for transfers between devices, in_one_piece(): whole, at, outs = (lax.all_gather(both, axis, axis=dim, tiled=True), 0, [])  50.3 us
    all_to_all x1, waiting for transfers between devices, local(): lax.all_to_all(results, ('sp', 'tp'), split_axis=0, concat_axis=0, tiled=...  29.3 us
    all_to_all x1, waiting for transfers between devices, local(): lax.all_to_all(outbound, ('sp', 'tp'), split_axis=0, concat_axis=0, tiled...  23.8 us
    all_to_all x1, starting transfers between devices, local(): lax.all_to_all(outbound, ('sp', 'tp'), split_axis=0, concat_axis=0, tiled...  11.5 us
    slice x2, local copies, waits for them, and re-layouts, in_one_piece(): outs.append(lax.slice_in_dim(whole, at, at + a.shape[along], axis=along))  7.53 us
    dot_general x1, matrix products, local(): jnp.einsum('sech,ehd->secd', hidden, expert_down, preferred_element_type=...  7.08 us
    all_to_all x1, starting transfers between devices, local(): lax.all_to_all(results, ('sp', 'tp'), split_axis=0, concat_axis=0, tiled=...  6.05 us
  transfers between devices with their start and end apart: 5, of which 4 were waited for; matrix products, arithmetic and copies ran while one was open for 10% of the time, Pallas kernels for 0%

commit v1 on v0

v1 whole, which is shorter than its diff:
```python
import math

import jax
import jax.numpy as jnp
from jax import lax
from jax.experimental import pallas as pl
from jax.experimental.pallas import tpu as pltpu
from jax.sharding import PartitionSpec as P

norm_epsilon = 1e-06


MESH = pl.DeviceIdType.MESH
LOG2E = math.log2(math.e)


def flash_heads(q_ref, kv, gate_rows, m_ref, l_ref, acc_ref, heads, size, diagonal):
    keys = kv[:, :size]
    values = kv[:, size:]
    rows = q_ref.shape[0] * q_ref.shape[1]
    length = keys.shape[0]
    scale = size ** (-0.5) * LOG2E
    for h in range(heads):
        q = q_ref[:, :, h * size : (h + 1) * size].reshape(rows, size)
        s = lax.dot_general(q, keys, (((1,), (1,)), ((), ())), preferred_element_type=jnp.float32)
        s = s * scale - gate_rows[h : h + 1, :]
        if diagonal:
            at = lax.broadcasted_iota(jnp.int32, (rows, length), 0)
            to = lax.broadcasted_iota(jnp.int32, (rows, length), 1)
            s = jnp.where(to <= at, s, -jnp.inf)
        top = jnp.broadcast_to(jnp.max(s, axis=1, keepdims=True), (rows, 128))
        if not diagonal:
            before = m_ref[h]
            top = jnp.maximum(before, top)
        p = jnp.exp2(s - jnp.concatenate([top] * (length // 128), axis=1))
        total = jnp.broadcast_to(jnp.sum(p, axis=1, keepdims=True), (rows, 128))
        out = jnp.dot(p.astype(jnp.bfloat16), values, preferred_element_type=jnp.float32)
        if not diagonal:
            factor = jnp.exp2(before - top)
            total = total + l_ref[h] * factor
            out = out + acc_ref[h] * jnp.concatenate([factor] * (size // 128), axis=1)
        m_ref[h] = top
        l_ref[h] = total
        acc_ref[h] = out


def attend_kernel(
    qn_in, kn_in, vn_in, gn_in, qb_in, kb_in, vb_in, gb_in, pn_in, pb_in, res_in, gain_in,
    stream_out, normed_out,
    nkv, bkv, qn, qb, attn, held, mn, ln, accn, mb, lb, accb, wn, wb, res, part, got,
    own_sem, load_sem, own_send, n1_send, n1_recv, b1_send, b1_recv, n2_send, n2_recv, b2_send,
    b2_recv, q_recv, swap_send, swap_recv, r_send, r_recv, a_send, a_recv,
):
    sp = lax.axis_index("sp")
    tp = lax.axis_index("tp")
    z = sp // 8
    y = (sp // 2) % 4
    c = sp % 2
    half = pl.ds(pl.multiple_of(c * 128, 128), 128)

    def at(zz, yy, cc):
        return (zz * 8 + yy * 2 + cc, tp)

    barrier = pltpu.get_barrier_semaphore()
    for step in range(1, 4):
        for cc in range(2):
            pl.semaphore_signal(barrier, inc=1, device_id=at(lax.rem(z + step, 4), y, cc), device_id_type=MESH)
            pl.semaphore_signal(barrier, inc=1, device_id=at(z, lax.rem(y + step, 4), cc), device_id_type=MESH)
        pl.semaphore_signal(barrier, inc=1, device_id=(sp, lax.rem(tp + step, 4)), device_id_type=MESH)
    pl.semaphore_signal(barrier, inc=1, device_id=at(z, y, 1 - c), device_id_type=MESH)

    weights = [
        pltpu.make_async_copy(pn_in, wn, load_sem.at[0]),
        pltpu.make_async_copy(pb_in, wb, load_sem.at[1]),
        pltpu.make_async_copy(res_in.at[pl.ds(pl.multiple_of(tp * 32, 32), 32)], res, load_sem.at[2]),
    ]
    for w in weights:
        w.start()
    pl.semaphore_wait(barrier, 16)

    def remote(src, dst, send, recv, to):
        return pltpu.make_async_remote_copy(
            src_ref=src, dst_ref=dst, send_sem=send, recv_sem=recv, device_id=to, device_id_type=MESH
        )

    nslot = ((kn_in, pl.ds(0, 128)), (vn_in, pl.ds(128, 128)))
    bslot = ((kb_in, pl.ds(0, 256)), (vb_in, pl.ds(256, 256)))

    def n_own(i):
        return nslot[i][0], nkv.at[z, y, half, nslot[i][1]]

    def b_own(i):
        return bslot[i][0], bkv.at[z, y, half, bslot[i][1]]

    n_pairs = [(lambda i=i: n_own(i)) for i in range(2)] + [lambda: (qn_in, qn.at[c])]
    b_pairs = [(lambda i=i: b_own(i)) for i in range(2)] + [lambda: (qb_in, qb.at[c])]

    for role, own, other in ((0, n_pairs, b_pairs), (1, b_pairs, n_pairs)):

        @pl.when(c == role)
        def _(own=own, other=other, role=role):
            for i in range(3):
                src, dst = other[i]()
                remote(src, dst, own_send.at[i], q_recv.at[i], at(z, y, 1 - role)).start()
            for i in range(3):
                src, dst = own[i]()
                pltpu.make_async_copy(src, dst, own_sem.at[i]).start()

    for step in range(1, 4):

        @pl.when(z + step < 4)
        def _(step=step):
            for i in range(2):
                src, dst = n_own(i)
                remote(src, dst, n1_send.at[step, i], n1_recv.at[z, c, i], at(z + step, y, 0)).start()

        for i in range(2):
            src, dst = b_own(i)
            remote(
                src, dst, b1_send.at[step, i], b1_recv.at[y, c, i], at(z, lax.rem(y + step, 4), 1)
            ).start()

    def own_wait(role, own, other):
        for i in range(3):
            src, dst = own[i]()
            pltpu.make_async_copy(src, dst, own_sem.at[i]).wait()
        oc = 1 - role
        ohalf = pl.ds(oc * 128, 128)
        if role == 0:
            dsts = [nkv.at[z, y, ohalf, nslot[i][1]] for i in range(2)] + [qn.at[oc]]
            srcs = [kn_in, vn_in, qn_in]
        else:
            dsts = [bkv.at[z, y, ohalf, bslot[i][1]] for i in range(2)] + [qb.at[oc]]
            srcs = [kb_in, vb_in, qb_in]
        for i in range(3):
            remote(srcs[i], dsts[i], own_send.at[i], q_recv.at[i], at(z, y, oc)).wait_recv()

    @pl.when(c == 0)
    def _():
        own_wait(0, n_pairs, b_pairs)

        def n2(zz, step, yy=None):
            to = y + step if yy is None else yy
            return remote(
                nkv.at[zz, y], nkv.at[zz, y], n2_send.at[zz, step], n2_recv.at[zz, y],
                at(z, lax.rem(y + step, 4), 0),
            )

        def send_on(zz):
            for step in range(1, 4):
                @pl.when((zz < z) | (y + step < 4))
                def _(step=step):
                    n2(zz, step).start()

        def block(zz, yy, diagonal):
            flash_heads(
                qn, nkv[zz, yy], gn_in[zz * 4 + yy], mn, ln, accn, 4, 128, diagonal
            )

        send_on(z)
        block(z, y, True)

        def column(t, carry):
            zz = z - t
            for cc in range(2):
                for i in range(2):
                    remote(
                        nslot[i][0], nkv.at[zz, y, pl.ds(cc * 128, 128), nslot[i][1]],
                        n1_send.at[1, i], n1_recv.at[zz, cc, i], at(zz, y, 0),
                    ).wait_recv()
            send_on(zz)
            block(zz, y, False)
            return carry

        lax.fori_loop(1, z + 1, column, 0)

        def rest(t, carry):
            zz = z - t // 3
            yy = lax.rem(y + t % 3 + 1, 4)

            @pl.when((zz < z) | (yy < y))
            def _():
                remote(
                    nkv.at[zz, yy], nkv.at[zz, yy], n2_send.at[zz, 1], n2_recv.at[zz, yy],
                    at(z, yy, 0),
                ).wait_recv()
                block(zz, yy, False)

            return carry

        lax.fori_loop(0, 3 * (z + 1), rest, 0)
        for h in range(4):
            out = (accn[h] / ln[h]).astype(jnp.bfloat16)
            held[:, :, h * 128 : (h + 1) * 128] = out.reshape(2, 128, 128)
        remote(
            held.at[1], attn.at[0], swap_send, swap_recv, at(z, y, 1)
        ).start()
        attn[0] = held[0]

        def drain(t, carry):
            for step in range(1, 4):
                @pl.when((t < z) | (y + step < 4))
                def _(step=step):
                    n2(t, step).wait_send()
            return carry

        lax.fori_loop(0, z + 1, drain, 0)

    @pl.when(c == 1)
    def _():
        own_wait(1, b_pairs, n_pairs)

        def b2(yy, step):
            return remote(
                bkv.at[z, yy], bkv.at[z, yy], b2_send.at[yy, step], b2_recv.at[z, yy],
                at(z + step, y, 1),
            )

        def send_on(yy):
            for step in range(1, 4):
                @pl.when(z + step < 4)
                def _(step=step):
                    b2(yy, step).start()

        def block(zz, yy, diagonal):
            flash_heads(qb, bkv[zz, yy], gb_in[zz * 4 + yy], mb, lb, accb, 2, 256, diagonal)

        send_on(y)
        block(z, y, True)

        def row(t, carry):
            yy = lax.rem(y + t, 4)
            for cc in range(2):
                for i in range(2):
                    remote(
                        bslot[i][0], bkv.at[z, yy, pl.ds(cc * 128, 128), bslot[i][1]],
                        b1_send.at[1, i], b1_recv.at[yy, cc, i], at(z, yy, 1),
                    ).wait_recv()
            send_on(yy)

            @pl.when(yy < y)
            def _():
                block(z, yy, False)

            return carry

        lax.fori_loop(1, 4, row, 0)

        def rest(t, carry):
            zz = z - 1 - t // 4
            yy = lax.rem(y + t, 4)
            remote(
                bkv.at[zz, yy], bkv.at[zz, yy], b2_send.at[yy, 1], b2_recv.at[zz, yy], at(zz, y, 1)
            ).wait_recv()
            block(zz, yy, False)
            return carry

        lax.fori_loop(0, 4 * z, rest, 0)
        for h in range(2):
            out = (accb[h] / jnp.concatenate([lb[h]] * 2, axis=1)).astype(jnp.bfloat16)
            held[:, :, h * 256 : (h + 1) * 256] = out.reshape(2, 128, 256)
        remote(
            held.at[0], attn.at[1], swap_send, swap_recv, at(z, y, 0)
        ).start()
        attn[1] = held[1]

        def drain(t, carry):
            for step in range(1, 4):
                @pl.when(z + step < 4)
                def _(step=step):
                    b2(t, step).wait_send()
            return carry

        lax.fori_loop(0, 4, drain, 0)

    for i in range(3):
        src, dst = n_pairs[i]() if i < 2 else n_pairs[2]()

        @pl.when(c == 1)
        def _(i=i):
            src, dst = n_pairs[i]()
            remote(src, dst, own_send.at[i], q_recv.at[i], at(z, y, 0)).wait_send()

        @pl.when(c == 0)
        def _(i=i):
            src, dst = b_pairs[i]()
            remote(src, dst, own_send.at[i], q_recv.at[i], at(z, y, 1)).wait_send()

    for step in range(1, 4):

        @pl.when(z + step < 4)
        def _(step=step):
            for i in range(2):
                src, dst = n_own(i)
                remote(src, dst, n1_send.at[step, i], n1_recv.at[z, c, i], at(z + step, y, 0)).wait_send()

        for i in range(2):
            src, dst = b_own(i)
            remote(
                src, dst, b1_send.at[step, i], b1_recv.at[y, c, i], at(z, lax.rem(y + step, 4), 1)
            ).wait_send()

    remote(held.at[1 - c], attn.at[1 - c], swap_send, swap_recv, at(z, y, 1 - c)).wait()
    for w in weights:
        w.wait()

    CH = 1024
    NC = 4096 // CH

    def sent(n, step):
        to = lax.rem(tp + step, 4)
        return remote(
            part.at[n, to], got.at[n, tp], r_send.at[n, step], r_recv.at[n, tp], (sp, to)
        )

    for n in range(NC):
        cols = pl.ds(n * CH, CH)
        p = jnp.dot(attn[0], wn[:, cols], preferred_element_type=jnp.float32)
        p = p + jnp.dot(attn[1], wb[:, cols], preferred_element_type=jnp.float32)
        part[n] = p.astype(jnp.bfloat16).reshape(4, 32, CH)
        for step in range(1, 4):
            sent(n, step).start()

    squares = jnp.zeros((32, 128), jnp.float32)
    for n in range(NC):
        for step in range(1, 4):
            frm = lax.rem(tp + step, 4)
            remote(
                part.at[n, frm], got.at[n, frm], r_send.at[n, step], r_recv.at[n, frm], (sp, frm)
            ).wait_recv()
        cols = pl.ds(n * CH, CH)
        total = res[:, cols].astype(jnp.float32) + part[n, tp].astype(jnp.float32)
        for step in range(1, 4):
            total = total + got[n, lax.rem(tp + step, 4)].astype(jnp.float32)
        stream_out[:, cols] = total
        sq = total * total
        for k in range(CH // 128):
            squares = squares + sq[:, k * 128 : (k + 1) * 128]
    mean = jnp.sum(squares, axis=1, keepdims=True) * (1.0 / 4096)
    rate = lax.rsqrt(mean + norm_epsilon)
    mine = pl.ds(pl.multiple_of(tp * 32, 32), 32)
    for n in range(NC):
        cols = pl.ds(n * CH, CH)
        normed_out[mine, cols] = (stream_out[:, cols] * rate * gain_in[:, cols]).astype(jnp.bfloat16)
    for step in range(1, 4):
        to = lax.rem(tp + step, 4)
        remote(
            normed_out.at[mine], normed_out.at[mine], a_send.at[step], a_recv.at[tp], (sp, to)
        ).start()
    for step in range(1, 4):
        frm = lax.rem(tp + step, 4)
        theirs = pl.ds(pl.multiple_of(frm * 32, 32), 32)
        remote(
            normed_out.at[theirs], normed_out.at[theirs], a_send.at[step], a_recv.at[frm], (sp, frm)
        ).wait_recv()
    for step in range(1, 4):
        to = lax.rem(tp + step, 4)
        remote(
            normed_out.at[mine], normed_out.at[mine], a_send.at[step], a_recv.at[tp], (sp, to)
        ).wait_send()
    for n in range(NC):
        for step in range(1, 4):
            sent(n, step).wait_send()


def attend(qn, kn, vn, gn, qb, kb, vb, gb, pn, pb, residual, gain):
    any_ = pl.BlockSpec(memory_space=pl.ANY)
    vm = pl.BlockSpec(memory_space=pltpu.VMEM)
    dma = pltpu.SemaphoreType.DMA
    f32, b16 = jnp.float32, jnp.bfloat16

    def rows(g):
        return (g * LOG2E).T.reshape(g.shape[1], 16, 256).transpose(1, 0, 2)

    return pl.pallas_call(
        attend_kernel,
        out_shape=(
            jax.ShapeDtypeStruct((32, 4096), f32),
            jax.ShapeDtypeStruct((128, 4096), b16),
        ),
        in_specs=[any_, any_, any_, vm, any_, any_, any_, vm, any_, any_, any_, vm],
        out_specs=(vm, vm),
        scratch_shapes=[
            pltpu.VMEM((4, 4, 256, 256), b16),
            pltpu.VMEM((4, 4, 256, 512), b16),
            pltpu.VMEM((2, 128, 512), b16),
            pltpu.VMEM((2, 128, 512), b16),
            pltpu.VMEM((2, 128, 512), b16),
            pltpu.VMEM((2, 128, 512), b16),
            pltpu.VMEM((4, 256, 128), f32),
            pltpu.VMEM((4, 256, 128), f32),
            pltpu.VMEM((4, 256, 128), f32),
            pltpu.VMEM((2, 256, 128), f32),
            pltpu.VMEM((2, 256, 128), f32),
            pltpu.VMEM((2, 256, 256), f32),
            pltpu.VMEM((512, 4096), b16),
            pltpu.VMEM((512, 4096), b16),
            pltpu.VMEM((32, 4096), b16),
            pltpu.VMEM((4, 4, 32, 1024), b16),
            pltpu.VMEM((4, 4, 32, 1024), b16),
            dma((3,)), dma((3,)), dma((3,)),
            dma((4, 2)), dma((4, 2, 2)), dma((4, 2)), dma((4, 2, 2)),
            dma((4, 4)), dma((4, 4)), dma((4, 4)), dma((4, 4)),
            dma((3,)), dma(()), dma(()),
            dma((4, 4)), dma((4, 4)), dma((4,)), dma((4,)),
        ],
        compiler_params=pltpu.CompilerParams(
            collective_id=0, has_side_effects=True, vmem_limit_bytes=48 * 2**20
        ),
        cost_estimate=pl.CostEstimate(flops=4 * 10**9, bytes_accessed=12 * 2**20, transcendentals=3 * 10**6),
        name="attend",
    )(qn, kn, vn, rows(gn), qb, kb, vb, rows(gb), pn, pb, residual, gain.reshape(1, -1))


def split_up(shard, dim, length):
    dims = shard.shape
    parts = shard.reshape(*dims[:dim], length, dims[dim] // length, *dims[dim + 1 :])
    return jnp.moveaxis(parts, dim, 0)


def sum_at_owner(shard, axis, dim):
    length = lax.axis_size(axis)
    parts = lax.all_to_all(split_up(shard, dim, length), axis, 0, 0, tiled=True)
    return jnp.sum(parts.astype(jnp.float32), axis=0)


def local(
    query_narrow,
    key_narrow,
    value_narrow,
    gates_narrow,
    query_broad,
    key_broad,
    value_broad,
    gates_broad,
    project_narrow,
    project_broad,
    residual,
    norm_gain,
    route_ids,
    route_weight,
    expert_gate,
    expert_up,
    expert_down,
    shared_gate,
    shared_up,
    shared_down,
):
    own_stream, normed = attend(
        query_narrow, key_narrow, value_narrow, gates_narrow,
        query_broad, key_broad, value_broad, gates_broad,
        project_narrow, project_broad, residual, norm_gain,
    )
    shared_hidden = (
        jax.nn.silu(jnp.dot(normed, shared_gate, preferred_element_type=jnp.float32))
        * jnp.dot(normed, shared_up, preferred_element_type=jnp.float32)
    ).astype(jnp.bfloat16)
    sub_rows = route_ids.shape[0]
    own_first = lax.axis_index("tp") * sub_rows
    shared = sum_at_owner(
        jnp.dot(shared_hidden, shared_down, preferred_element_type=jnp.float32).astype(
            jnp.bfloat16
        ),
        "tp",
        0,
    )
    top_count = route_ids.shape[1]
    local_experts = expert_gate.shape[0]
    expert_total = lax.axis_size("sp") * lax.axis_size("tp") * local_experts
    capacity = 2 * sub_rows * top_count // expert_total
    flat_ids = route_ids.reshape(-1)
    one_hot = (flat_ids[:, None] == jnp.arange(expert_total, dtype=jnp.int32)[None, :]).astype(
        jnp.int32
    )
    slot_of = jnp.sum(one_hot * (jnp.cumsum(one_hot, axis=0) - 1), axis=1)
    target = (flat_ids * capacity + slot_of).reshape(sub_rows, top_count)
    slot_total = expert_total * capacity
    matches = target[None, :, :] == jnp.arange(slot_total, dtype=jnp.int32)[:, None, None]
    dispatch = jnp.any(matches, axis=-1).astype(jnp.bfloat16)
    own_normed = lax.dynamic_slice_in_dim(normed, own_first, sub_rows, 0)
    outbound = (
        jnp.dot(dispatch, own_normed, preferred_element_type=jnp.float32)
        .astype(jnp.bfloat16)
        .reshape(expert_total, capacity, -1)
    )
    weight_rounded = route_weight.astype(jnp.bfloat16)
    combiner = jnp.sum(
        jnp.where(matches, weight_rounded[None], jnp.zeros((), jnp.bfloat16)), axis=-1
    ).T
    inbound = lax.all_to_all(outbound, ("sp", "tp"), split_axis=0, concat_axis=0, tiled=True)
    senders = inbound.shape[0] // local_experts
    grouped = inbound.reshape(senders, local_experts, inbound.shape[1], inbound.shape[2])
    gate_out = jnp.einsum(
        "secd,edh->sech", grouped, expert_gate, preferred_element_type=jnp.float32
    )
    up_out = jnp.einsum("secd,edh->sech", grouped, expert_up, preferred_element_type=jnp.float32)
    hidden = (jax.nn.silu(gate_out) * up_out).astype(jnp.bfloat16)
    result = jnp.einsum(
        "sech,ehd->secd", hidden, expert_down, preferred_element_type=jnp.float32
    ).astype(jnp.bfloat16)
    results = result.reshape(inbound.shape)
    returned = lax.all_to_all(results, ("sp", "tp"), split_axis=0, concat_axis=0, tiled=True)
    routed = jnp.dot(combiner, returned.reshape(slot_total, -1), preferred_element_type=jnp.float32)
    return (own_stream + shared + routed).astype(jnp.bfloat16)


def solution(mesh):
    placed = (
        P("sp", "tp"),
        P("sp", "tp"),
        P("sp", "tp"),
        P(None, "tp"),
        P("sp", "tp"),
        P("sp", "tp"),
        P("sp", "tp"),
        P(None, "tp"),
        P("tp", None),
        P("tp", None),
        P("sp", None),
        P(),
        P(("sp", "tp"), None),
        P(("sp", "tp"), None),
        P(("sp", "tp"), None, None),
        P(("sp", "tp"), None, None),
        P(("sp", "tp"), None, None),
        P(None, "tp"),
        P(None, "tp"),
        P("tp", None),
    )
    return jax.shard_map(
        local, mesh=mesh, in_specs=placed, out_specs=P(("sp", "tp"), None), check_vma=False
    )
```

time: 301 us -> 187 us (0.62)
  waiting for transfers between devices: 196 us -> 53.2 us
  Pallas kernels: 0 us -> 50.7 us
  between operations: 13.7 us -> 0.14 us
  starting transfers between devices: 21.3 us -> 32.1 us
  matrix products: 33.2 us -> 23.8 us
  local copies, waits for them, and re-layouts: 27.3 us -> 22.5 us
  other arithmetic: 7.44 us -> 3.91 us
    psum x1 -> x0, waiting for transfers between devices: 92.1 us -> none  [local(): lax.psum(partial_value.astype(jnp.bfloat16), 'tp').astype(jnp.float32)]
    pallas_call x0 -> x1, Pallas kernels: none -> 50.7 us  [attend(): pl.pallas_call(attend_kernel, out_shape=(jax.ShapeDtypeStruct((32, 4096),...]
    all_gather x1 -> x0, waiting for transfers between devices: 50.3 us -> none  [in_one_piece(): whole, at, outs = (lax.all_gather(both, axis, axis=dim, tiled=True), 0, [])]
    all_to_all x1, starting transfers between devices: 11.5 us -> 22.4 us  [local(): lax.all_to_all(outbound, ('sp', 'tp'), split_axis=0, concat_axis=0, tiled...]
    dot_general x6 -> x0, matrix products: 10 us -> none  [the longest x1 3.08 us: local(): jnp.dot(heads_out[0], project_narrow, preferred_element_type=jnp.float32)]
    slice x2 -> x0, local copies, waits for them, and re-layouts: 7.53 us -> none  [in_one_piece(): outs.append(lax.slice_in_dim(whole, at, at + a.shape[along], axis=along))]
    unnamed x23 -> x27, local copies, waits for them, and re-layouts: 2.78 us -> 8.66 us
    add x5 -> x0, other arithmetic: 3.1 us -> none  [the longest x1 3.06 us: local(): stream = residual.astype(jnp.float32) + mixture]
  transfers between devices with their start and end apart: 5 -> 3, of which waited for: 4 -> 2; matrix products, arithmetic and copies ran while one was open for 10% -> 13% of each run, Pallas kernels for 0% -> 0%
where the time goes in v1:
time: 187 us; the launch traced here: 186 us
  waiting for transfers between devices  53.2 us (28%)
  Pallas kernels  50.7 us (27%)
  starting transfers between devices  32.1 us (17%)
  matrix products  23.8 us (13%)
  local copies, waits for them, and re-layouts  22.5 us (12%)
  other arithmetic  3.91 us (2%)
    pallas_call x1, Pallas kernels, attend(): pl.pallas_call(attend_kernel, out_shape=(jax.ShapeDtypeStruct((32, 4096),...  50.7 us
    all_to_all x1, waiting for transfers between devices, local(): lax.all_to_all(results, ('sp', 'tp'), split_axis=0, concat_axis=0, tiled=...  29.3 us
    all_to_all x1, waiting for transfers between devices, local(): lax.all_to_all(outbound, ('sp', 'tp'), split_axis=0, concat_axis=0, tiled...  23.8 us
    all_to_all x1, starting transfers between devices, local(): lax.all_to_all(outbound, ('sp', 'tp'), split_axis=0, concat_axis=0, tiled...  22.4 us
    unnamed x27, local copies, waits for them, and re-layouts  8.66 us
    dot_general x1, matrix products, local(): jnp.einsum('sech,ehd->secd', hidden, expert_down, preferred_element_type=...  7.05 us
    all_to_all x1, starting transfers between devices, local(): lax.all_to_all(results, ('sp', 'tp'), split_axis=0, concat_axis=0, tiled=...  6.05 us
    dot_general x1, matrix products, local(): jnp.einsum('secd,edh->sech', grouped, expert_gate, preferred_element_type...  5.34 us
  transfers between devices with their start and end apart: 3, of which 2 were waited for; matrix products, arithmetic and copies ran while one was open for 13% of the time, Pallas kernels for 0%

profile of v1, /device:TPU:1, one launch (start us, length us, event | category | flops | bytes accessed | tf_op | source)
XLA Modules:
  0.0 186.3 jit_solution(12247845506471654090)
XLA Ops:
  0.0 0.0 copy-start
  0.0 0.9 copy.46
  0.9 0.1 eq.28
  1.0 0.8 broadcast_multiply_fusion.1
  1.8 0.1 fusion.53
  1.9 0.2 reduce_window_sum.11
  2.1 0.2 select_reduce_fusion
  2.2 0.1 reduce_sum.34
  2.4 0.1 copy.47
  2.4 0.7 multiply_add_fusion
  3.1 0.1 fusion.45
  3.2 0.9 broadcast_multiply_fusion
  4.1 0.0 copy-start.3
  4.1 1.2 copy-done.3
  5.3 0.0 copy-start.4
  5.3 0.9 copy-done.4
  6.2 0.0 copy-start.5
  6.2 0.9 copy-done.5
  7.1 0.0 copy-start.6
  7.1 0.8 copy-done.6
  8.0 0.8 copy-done.7
  8.8 0.8 copy-done.8
  9.6 0.8 copy-done.9
  10.3 0.7 copy-done.10
  11.0 50.7 %attend.1 = (f32[32,4096]{1,0:T(8,128)S(1)}, bf16[128,4096]{1,0:T(8,128)(2,1)S(1)}) custom-call(bf16[128,512]{1,0:T(8,128)(2,1)S(1)} %copy-done.4, bf16[128,128]{1,0:T(8,128)(2,1)S(1)} %copy-done.8, bf16[128,128]{1,0:T(8,128)(2,1)S(1)} %copy-done.9, f32[16,4,256]{2,1,0:T(4,128)S(1)} %bitcast.68, bf16[128,512]{1,0:T(8,128)(2,1)S(1)} %copy-done.5, ...), custom_call_target="tpu_custom_call" | custom-call | flops 4000000000 | bytes 12582912 | tf_op jit(solution)/shard_map/attend/pallas_call | solution.py:375
  61.7 0.0 copy-start.1
  61.7 0.8 copy-done.1
  62.5 2.1 %convolution_convert_fusion.1 = bf16[256,4096]{1,0:T(8,128)(2,1)} fusion(pred[256,32]{0,1:T(8,128)(4,1)S(1)} %fusion.45, bf16[128,4096]{1,0:T(8,128)(2,1)S(1)} %get-tuple-element.8, s32[]{:T(128)S(6)} %select_n.8), kind=kOutput, calls=%fused_computation.1 | convolution fusion | flops 68157440 | bytes 2367492 | tf_op jit(solution)/shard_map/dot_general | solution.py:482
  64.6 4.4 %reshape.53 = bf16[128,2,4096]{2,1,0:T(2,128)(2,1)} reshape(bf16[256,4096]{1,0:T(8,128)(2,1)} %convolution_convert_fusion.1) | data formatting | bytes 4194304 | tf_op jit(solution)/shard_map/reshape | solution.py:484
  69.0 22.4 %all-to-all-start.1 = ((bf16[128,2,4096]{2,1,0:T(2,128)(2,1)}), bf16[128,2,4096]{2,1,0:T(2,128)(2,1)}, u32[]{:S(2)}, u32[]{:S(2)}) async-start(bf16[128,2,4096]{2,1,0:T(2,128)(2,1)} %reshape.53), calls=%async_computation.1 | async-start | bytes 4194304 | tf_op jit(solution)/shard_map/all_to_all | solution.py:490
  91.4 2.0 %fusion.58 = f32[128,256]{1,0:T(8,128)S(1)} fusion(bf16[128,4096]{1,0:T(8,128)(2,1)S(1)} %get-tuple-element.8, bf16[4096,256]{1,0:T(8,128)(2,1)} %param.37), kind=kOutput, calls=%fused_computation.46 | convolution fusion | flops 268435456 | bytes 3276800 | tf_op jit(solution)/shard_map/dot_general | solution.py:455
  93.4 4.5 %convolution_convert_fusion.2 = bf16[128,4096]{1,0:T(8,128)(2,1)} fusion(bf16[256,4096]{1,0:T(8,128)(2,1)} %param.39, bf16[128,4096]{1,0:T(8,128)(2,1)S(1)} %get-tuple-element.8, bf16[4096,256]{1,0:T(8,128)(2,1)} %param.38, f32[128,256]{1,0:T(8,128)S(1)} %fusion.58), kind=kOutput, calls=%fused_computation.2 | convolution fusion | flops 537591808 | bytes 6422528 | tf_op jit(solution)/shard_map/dot_general | solution.py:461
  98.0 23.8 %all-to-all-done.1 = bf16[128,2,4096]{2,1,0:T(2,128)(2,1)} async-done(((bf16[128,2,4096]{2,1,0:T(2,128)(2,1)}), bf16[128,2,4096]{2,1,0:T(2,128)(2,1)}, u32[]{:S(2)}, u32[]{:S(2)}) %all-to-all-start.1) | async-done | bytes 2097184 | tf_op jit(solution)/shard_map/all_to_all | solution.py:490
  121.8 3.7 %all-to-all-start = ((bf16[4,32,4096]{2,1,0:T(8,128)(2,1)}), bf16[4,32,4096]{2,1,0:T(8,128)(2,1)S(1)}, u32[]{:S(2)}, u32[]{:S(2)}) async-start(bf16[4,32,4096]{2,1,0:T(8,128)(2,1)} %bitcast.71), calls=%async_computation | async-start | bytes 2097152 | tf_op jit(solution)/shard_map/all_to_all | solution.py:423
  125.5 5.3 %fusion.8 = f32[128,1,2,256]{3,0,2,1:T(8,128)} fusion(bf16[1,4096,256]{2,1,0:T(8,128)(2,1)} %param.34, bf16[128,2,4096]{2,1,0:T(2,128)(2,1)} %all-to-all-done.1), kind=kOutput, calls=%fused_computation.13 | convolution fusion | flops 536870912 | bytes 4456448 | tf_op jit(solution)/shard_map/secd,edh->sech/dot_general | solution.py:493
  130.8 0.0 copy-done
  130.8 7.1 %convolution_convert_fusion = bf16[128,2,4096]{2,0,1:T(8,128)(2,1)} fusion(bf16[1,256,4096]{2,1,0:T(8,128)(2,1)S(1)} %copy-done, bf16[1,4096,256]{2,1,0:T(8,128)(2,1)} %param.35, bf16[128,2,4096]{2,1,0:T(2,128)(2,1)} %all-to-all-done.1, f32[128,1,2,256]{3,0,2,1:T(8,128)} %fusion.8), kind=kOutput, calls=%fused_computation | convolution fusion | flops 1075183616 | bytes 8650752 | tf_op jit(solution)/shard_map/sech,ehd->secd/dot_general | solution.py:498
  137.9 5.1 %copy.50 = bf16[128,2,4096]{2,1,0:T(2,128)(2,1)} copy(bf16[128,2,4096]{2,0,1:T(8,128)(2,1)} %convolution_convert_fusion) | data formatting | bytes 4194304 | tf_op jit(solution)/shard_map/convert_element_type | solution.py:500
  143.0 0.0 all-to-all-done
  143.0 6.0 %all-to-all-start.2 = ((bf16[128,2,4096]{2,1,0:T(2,128)(2,1)}), bf16[128,2,4096]{2,1,0:T(2,128)(2,1)}, u32[]{:S(2)}, u32[]{:S(2)}) async-start(bf16[128,2,4096]{2,1,0:T(2,128)(2,1)} %copy.50), calls=%async_computation.2 | async-start | bytes 4194304 | tf_op jit(solution)/shard_map/all_to_all | solution.py:502
  149.1 0.0 copy-done.12
  149.1 0.1 fusion.52
  149.2 1.0 convert_reduce_fusion
  150.2 29.3 %all-to-all-done.2 = bf16[128,2,4096]{2,1,0:T(2,128)(2,1)} async-done(((bf16[128,2,4096]{2,1,0:T(2,128)(2,1)}), bf16[128,2,4096]{2,1,0:T(2,128)(2,1)}, u32[]{:S(2)}, u32[]{:S(2)}) %all-to-all-start.2) | async-done | bytes 2097184 | tf_op jit(solution)/shard_map/all_to_all | solution.py:502
  179.5 4.1 %reshape.58 = bf16[256,4096]{1,0:T(8,128)(2,1)} reshape(bf16[128,2,4096]{2,1,0:T(2,128)(2,1)} %all-to-all-done.2) | data formatting | bytes 4194304 | tf_op jit(solution)/shard_map/reshape | solution.py:503
  183.6 0.0 copy-done.2
  183.6 0.0 copy-done.11
  183.6 2.8 %fusion = bf16[32,4096]{1,0:T(8,128)(2,1)} fusion(bf16[256,32]{0,1:T(8,128)(2,1)S(1)} %fusion.52, bf16[256,4096]{1,0:T(8,128)(2,1)} %reshape.58, f32[32,4096]{1,0:T(8,128)S(1)} %copy-done.2, f32[32,4096]{1,0:T(8,128)S(1)} %copy-done.11), kind=kOutput, calls=%fused_computation.4 | convolution fusion | flops 67502080 | bytes 3424256 | tf_op jit(solution)/shard_map/dot_general | solution.py:503
  (8 shorter events, 0.0 us)
Async XLA Ops:
  0.0 130.8 %copy-start = (bf16[1,256,4096]{2,1,0:T(8,128)(2,1)S(1)}, bf16[1,256,4096]{2,1,0:T(8,128)(2,1)}, u32[]{:S(2)}) copy-start(bf16[1,256,4096]{2,1,0:T(8,128)(2,1)} %param.36) | copy-start | bytes 6291460
  4.1 1.2 copy-start.3
  5.3 0.9 copy-start.4
  6.2 0.9 copy-start.5
  7.1 0.8 copy-start.6
  8.0 0.8 copy-start.7
  8.8 0.8 copy-start.8
  9.6 0.8 copy-start.9
  10.3 0.7 copy-start.10
  61.7 0.8 copy-start.1
  69.0 52.8 %all-to-all-start.1 = ((bf16[128,2,4096]{2,1,0:T(2,128)(2,1)}), bf16[128,2,4096]{2,1,0:T(2,128)(2,1)}, u32[]{:S(2)}, u32[]{:S(2)}) async-start(bf16[128,2,4096]{2,1,0:T(2,128)(2,1)} %reshape.53), calls=%async_computation.1 | async-start | bytes 4194304 | tf_op jit(solution)/shard_map/all_to_all | solution.py:490
  121.8 21.2 %all-to-all-start = ((bf16[4,32,4096]{2,1,0:T(8,128)(2,1)}), bf16[4,32,4096]{2,1,0:T(8,128)(2,1)S(1)}, u32[]{:S(2)}, u32[]{:S(2)}) async-start(bf16[4,32,4096]{2,1,0:T(8,128)(2,1)} %bitcast.71), calls=%async_computation | async-start | bytes 2097152 | tf_op jit(solution)/shard_map/all_to_all | solution.py:423
  143.0 6.1 %copy-start.12 = (f32[32,4]{0,1:T(4,128)S(1)}, f32[32,4]{0,1:T(4,128)}, u32[]{:S(2)}) copy-start(f32[32,4]{0,1:T(4,128)} %param.33) | copy-start | bytes 1540
  143.0 36.5 %all-to-all-start.2 = ((bf16[128,2,4096]{2,1,0:T(2,128)(2,1)}), bf16[128,2,4096]{2,1,0:T(2,128)(2,1)}, u32[]{:S(2)}, u32[]{:S(2)}) async-start(bf16[128,2,4096]{2,1,0:T(2,128)(2,1)} %copy.50), calls=%async_computation.2 | async-start | bytes 4194304 | tf_op jit(solution)/shard_map/all_to_all | solution.py:502
  150.2 33.4 %copy-start.2 = (f32[32,4096]{1,0:T(8,128)S(1)}, f32[32,4096]{1,0:T(8,128)}, u32[]{:S(2)}) copy-start(f32[32,4096]{1,0:T(8,128)} %copy-done.1) | copy-start | bytes 1572868
  150.2 33.4 %copy-start.11 = (f32[32,4096]{1,0:T(8,128)S(1)}, f32[32,4096]{1,0:T(8,128)}, u32[]{:S(2)}) copy-start(f32[32,4096]{1,0:T(8,128)} %convert_reduce_fusion) | copy-start | bytes 1572868

commit v2 on v1

--- a/solution.py
+++ b/solution.py
@@ -8,7 +8,6 @@
 from jax.sharding import PartitionSpec as P
 
 norm_epsilon = 1e-06
-
 
 MESH = pl.DeviceIdType.MESH
 LOG2E = math.log2(math.e)
@@ -44,12 +43,16 @@
         acc_ref[h] = out
 
 
-def attend_kernel(
+def layer_kernel(
     qn_in, kn_in, vn_in, gn_in, qb_in, kb_in, vb_in, gb_in, pn_in, pb_in, res_in, gain_in,
-    stream_out, normed_out,
-    nkv, bkv, qn, qb, attn, held, mn, ln, accn, mb, lb, accb, wn, wb, res, part, got,
+    ids_in, rw_in, eg_in, eu_in, ed_in, sg_in, su_in, sd_in,
+    out_ref,
+    nkv, bkv, qn, qb, attn, held, mn, ln, accn, mb, lb, accb, wn, wb, res, part, got, stream, normed,
+    gn, gb, gain, ids, rw, wgu, wd, sgu, sd, codes, dmat, cmat, outb, inb, back, ret, gu, mine,
+    theirs, from_pair, part2, got2,
     own_sem, load_sem, own_send, n1_send, n1_recv, b1_send, b1_recv, n2_send, n2_recv, b2_send,
     b2_recv, q_recv, swap_send, swap_recv, r_send, r_recv, a_send, a_recv,
+    c_send, c_recv, p_send, p_recv, d_send, d_recv, e_send, e_recv, t_send, t_recv, s_send, s_recv,
 ):
     sp = lax.axis_index("sp")
     tp = lax.axis_index("tp")
@@ -62,21 +65,37 @@
         return (zz * 8 + yy * 2 + cc, tp)
 
     barrier = pltpu.get_barrier_semaphore()
+
+    def greet(to):
+        pl.semaphore_signal(barrier, inc=1, device_id=to, device_id_type=MESH)
+
+    def greet_chip(t, carry):
+        greet(at(lax.rem(z + t // 4, 4), lax.rem(y + t % 4, 4), c))
+        return carry
+
+    lax.fori_loop(1, 16, greet_chip, 0)
     for step in range(1, 4):
+        greet(at(lax.rem(z + step, 4), y, 1 - c))
+        greet(at(z, lax.rem(y + step, 4), 1 - c))
         for cc in range(2):
-            pl.semaphore_signal(barrier, inc=1, device_id=at(lax.rem(z + step, 4), y, cc), device_id_type=MESH)
-            pl.semaphore_signal(barrier, inc=1, device_id=at(z, lax.rem(y + step, 4), cc), device_id_type=MESH)
-        pl.semaphore_signal(barrier, inc=1, device_id=(sp, lax.rem(tp + step, 4)), device_id_type=MESH)
-    pl.semaphore_signal(barrier, inc=1, device_id=at(z, y, 1 - c), device_id_type=MESH)
-
-    weights = [
-        pltpu.make_async_copy(pn_in, wn, load_sem.at[0]),
-        pltpu.make_async_copy(pb_in, wb, load_sem.at[1]),
-        pltpu.make_async_copy(res_in.at[pl.ds(pl.multiple_of(tp * 32, 32), 32)], res, load_sem.at[2]),
+            greet((z * 8 + y * 2 + cc, lax.rem(tp + step, 4)))
+    greet(at(z, y, 1 - c))
+
+    loads = [
+        (gn_in, gn), (gb_in, gb), (ids_in, ids), (rw_in, rw), (gain_in, gain),
+        (res_in.at[pl.ds(pl.multiple_of(tp * 32, 32), 32)], res),
+        (pn_in, wn), (pb_in, wb),
+        (sg_in, sgu.at[:, pl.ds(0, 256)]), (su_in, sgu.at[:, pl.ds(256, 256)]), (sd_in, sd),
+        (eg_in.at[0], wgu.at[:, pl.ds(0, 256)]), (eu_in.at[0], wgu.at[:, pl.ds(256, 256)]),
+        (ed_in.at[0], wd),
     ]
-    for w in weights:
-        w.start()
-    pl.semaphore_wait(barrier, 16)
+
+    def load(i):
+        return pltpu.make_async_copy(loads[i][0], loads[i][1], load_sem.at[i])
+
+    for i in range(len(loads)):
+        load(i).start()
+    pl.semaphore_wait(barrier, 28)
 
     def remote(src, dst, send, recv, to):
         return pltpu.make_async_remote_copy(
@@ -119,6 +138,43 @@
             remote(
                 src, dst, b1_send.at[step, i], b1_recv.at[y, c, i], at(z, lax.rem(y + step, 4), 1)
             ).start()
+
+    me = c * 4 + tp
+    for i in range(4):
+        load(i).wait()
+    lane = lax.broadcasted_iota(jnp.int32, (8, 128), 1)
+    row = lax.broadcasted_iota(jnp.int32, (32, 128), 0)
+    spot = (lax.broadcasted_iota(jnp.int32, (32, 128), 1) == row + tp * 32).astype(jnp.bfloat16)
+    put = lambda a: jnp.dot(a.astype(jnp.bfloat16), spot, preferred_element_type=jnp.float32)
+    placed_ids = put(ids[...].astype(jnp.float32))
+    placed_rw = put(rw[...])
+    inside = (lane[:4] // 32) == tp
+    key_ids = jnp.where(inside, placed_ids, -1.0)
+    names = lax.broadcasted_iota(jnp.int32, (128, 128), 0).astype(jnp.float32)
+    later = (
+        lax.broadcasted_iota(jnp.int32, (128, 128), 0) < lax.broadcasted_iota(jnp.int32, (128, 128), 1)
+    ).astype(jnp.bfloat16)
+    hits = [jnp.where(key_ids[k : k + 1] == names, 1.0, 0.0) for k in range(4)]
+    before = jnp.dot(
+        (hits[0] + hits[1] + hits[2] + hits[3]).astype(jnp.bfloat16), later,
+        preferred_element_type=jnp.float32,
+    )
+    for k in range(4):
+        rank = jnp.sum(hits[k] * before, axis=0, keepdims=True)
+        codes[me, k : k + 1] = placed_ids[k : k + 1] * 2.0 + rank
+        codes[me, 4 + k : 5 + k] = placed_rw[k : k + 1]
+
+    def code(t):
+        to = lax.rem(me + t, 8)
+        return remote(
+            codes.at[me], codes.at[me], c_send.at[t], c_recv.at[t], (z * 8 + y * 2 + to // 4, to % 4)
+        )
+
+    for t in range(1, 8):
+        code(t).start()
+
+    def gate_rows(ref, zz, yy):
+        return ref[:, pl.ds(pl.multiple_of((zz * 4 + yy) * 256, 256), 256)] * LOG2E
 
     def own_wait(role, own, other):
         for i in range(3):
@@ -154,7 +210,7 @@
 
         def block(zz, yy, diagonal):
             flash_heads(
-                qn, nkv[zz, yy], gn_in[zz * 4 + yy], mn, ln, accn, 4, 128, diagonal
+                qn, nkv[zz, yy], gate_rows(gn, zz, yy), mn, ln, accn, 4, 128, diagonal
             )
 
         send_on(z)
@@ -223,7 +279,7 @@
                     b2(yy, step).start()
 
         def block(zz, yy, diagonal):
-            flash_heads(qb, bkv[zz, yy], gb_in[zz * 4 + yy], mb, lb, accb, 2, 256, diagonal)
+            flash_heads(qb, bkv[zz, yy], gate_rows(gb, zz, yy), mb, lb, accb, 2, 256, diagonal)
 
         send_on(y)
         block(z, y, True)
@@ -301,8 +357,8 @@
             ).wait_send()
 
     remote(held.at[1 - c], attn.at[1 - c], swap_send, swap_recv, at(z, y, 1 - c)).wait()
-    for w in weights:
-        w.wait()
+    for i in range(4, 8):
+        load(i).wait()
 
     CH = 1024
     NC = 4096 // CH
@@ -332,176 +388,198 @@
         total = res[:, cols].astype(jnp.float32) + part[n, tp].astype(jnp.float32)
         for step in range(1, 4):
             total = total + got[n, lax.rem(tp + step, 4)].astype(jnp.float32)
-        stream_out[:, cols] = total
+        stream[:, cols] = total
         sq = total * total
         for k in range(CH // 128):
             squares = squares + sq[:, k * 128 : (k + 1) * 128]
     mean = jnp.sum(squares, axis=1, keepdims=True) * (1.0 / 4096)
     rate = lax.rsqrt(mean + norm_epsilon)
-    mine = pl.ds(pl.multiple_of(tp * 32, 32), 32)
+    rows_of = lambda who: pl.ds(pl.multiple_of(who * 32, 32), 32)
     for n in range(NC):
         cols = pl.ds(n * CH, CH)
-        normed_out[mine, cols] = (stream_out[:, cols] * rate * gain_in[:, cols]).astype(jnp.bfloat16)
+        normed[c, rows_of(tp), cols] = (stream[:, cols] * rate * gain[:, cols]).astype(jnp.bfloat16)
+
+    def gather(step):
+        to = lax.rem(tp + step, 4)
+        block = normed.at[c, rows_of(tp)]
+        return remote(block, block, a_send.at[step], a_recv.at[step], (sp, to))
+
+    def pair(who):
+        block = normed.at[c, rows_of(who)]
+        return remote(block, block, p_send.at[who], p_recv.at[who], at(z, y, 1 - c))
+
     for step in range(1, 4):
+        gather(step).start()
+    pair(tp).start()
+
+    for t in range(1, 8):
+        code(t).wait_recv()
+    halves = [codes[h * 4] + codes[h * 4 + 1] + codes[h * 4 + 2] + codes[h * 4 + 3] for h in range(2)]
+    table = jnp.concatenate(halves, axis=1)
+    slot = lax.broadcasted_iota(jnp.int32, (256, 256), 0)
+    token = lax.broadcasted_iota(jnp.int32, (256, 256), 1)
+    wanted = (((slot // 16) * 2 + c) * 4 + tp) * 2 + slot % 2
+    wanted = jnp.where((slot // 2) % 8 == token // 32, wanted, -1).astype(jnp.float32)
+    picks = jnp.zeros((256, 256), jnp.float32)
+    pays = jnp.zeros((256, 256), jnp.float32)
+    for k in range(4):
+        same = table[k : k + 1] == wanted
+        picks = picks + jnp.where(same, 1.0, 0.0)
+        pays = pays + jnp.where(same, table[4 + k : 5 + k], 0.0)
+    dmat[...] = picks.astype(jnp.bfloat16)
+    cmat[...] = pays.T.reshape(2, 128, 256).astype(jnp.bfloat16)
+
+    for step in range(1, 4):
+        gather(step).wait_recv()
+    for step in range(1, 4):
+        pair(lax.rem(tp + step, 4)).start()
+    for who in range(4):
+        block = normed.at[1 - c, pl.ds(who * 32, 32)]
+        remote(block, block, p_send.at[who], p_recv.at[who], at(z, y, 1 - c)).wait_recv()
+
+    chip = z * 4 + y
+
+    def slots(src, dst, send, recv, n):
+        def one(t, carry):
+            zz, yy = lax.rem(z + t // 4, 4), lax.rem(y + t % 4, 4)
+            remote(
+                src.at[n, zz * 4 + yy], dst.at[n, chip], send.at[n], recv.at[n], at(zz, yy, c)
+            ).start()
+            return carry
+
+        lax.fori_loop(1, 16, one, 0)
+
+    def all_of(ref, sem, n):
+        block = ref.at[n, pl.ds(0, 15)]
+        return pltpu.make_async_copy(block, block, sem.at[n])
+
+    for n in range(NC):
+        cols = pl.ds(n * CH, CH)
+        rows = normed[:, :, cols].reshape(256, CH)
+        picked = jnp.dot(dmat[...], rows, preferred_element_type=jnp.float32).astype(jnp.bfloat16)
+        outb[n] = picked.reshape(16, 16, CH)
+        slots(outb, inb, d_send, d_recv, n)
+        inb[n, chip] = outb[n, chip]
+
+    for i in range(8, 14):
+        load(i).wait()
+    both = jnp.dot(normed[c], sgu[...], preferred_element_type=jnp.float32)
+    gate, up = both[:, :256], both[:, 256:]
+    hidden = (gate / (1.0 + jnp.exp(-gate)) * up).astype(jnp.bfloat16)
+    for n in range(NC):
+        mine[n] = jnp.dot(hidden, sd[:, n * CH : (n + 1) * CH], preferred_element_type=jnp.float32)
+
+    for n in range(NC):
+        all_of(inb, d_recv, n).wait()
+        more = jnp.dot(
+            inb[n].reshape(256, CH), wgu[n * CH : (n + 1) * CH, :], preferred_element_type=jnp.float32
+        )
+        gu[...] = more if n == 0 else gu[...] + more
+    gate, up = gu[:, :256], gu[:, 256:]
+    hidden = (gate / (1.0 + jnp.exp(-gate)) * up).astype(jnp.bfloat16)
+    for n in range(NC):
+        made = jnp.dot(hidden, wd[:, n * CH : (n + 1) * CH], preferred_element_type=jnp.float32)
+        back[n] = made.astype(jnp.bfloat16).reshape(16, 16, CH)
+        slots(back, ret, e_send, e_recv, n)
+        ret[n, chip] = back[n, chip]
+
+    def to_pair(n):
+        return remote(theirs.at[n], from_pair.at[n], t_send.at[n], t_recv.at[n], at(z, y, 1 - c))
+
+    def to_owner(n, step):
         to = lax.rem(tp + step, 4)
-        remote(
-            normed_out.at[mine], normed_out.at[mine], a_send.at[step], a_recv.at[tp], (sp, to)
-        ).start()
+        return remote(
+            part2.at[n, to], got2.at[n, step], s_send.at[n, step], s_recv.at[n, step], (sp, to)
+        )
+
+    for i in range(NC + 2):
+        if i < NC:
+            all_of(ret, e_recv, i).wait()
+            rows = ret[i].reshape(256, CH)
+            theirs[i] = jnp.dot(cmat[1 - c], rows, preferred_element_type=jnp.float32).astype(
+                jnp.bfloat16
+            )
+            to_pair(i).start()
+            mine[i] = mine[i] + jnp.dot(cmat[c], rows, preferred_element_type=jnp.float32)
+        if 0 <= i - 1 < NC:
+            n = i - 1
+            to_pair(n).wait_recv()
+            both = mine[n] + from_pair[n].astype(jnp.float32)
+            part2[n] = both.astype(jnp.bfloat16).reshape(4, 32, CH)
+            for step in range(1, 4):
+                to_owner(n, step).start()
+        if 0 <= i - 2:
+            n = i - 2
+            for step in range(1, 4):
+                to_owner(n, step).wait_recv()
+            total = stream[:, n * CH : (n + 1) * CH] + part2[n, tp].astype(jnp.float32)
+            for step in range(1, 4):
+                total = total + got2[n, step].astype(jnp.float32)
+            out_ref[:, n * CH : (n + 1) * CH] = total.astype(jnp.bfloat16)
+
+    for t in range(1, 8):
+        code(t).wait_send()
     for step in range(1, 4):
-        frm = lax.rem(tp + step, 4)
-        theirs = pl.ds(pl.multiple_of(frm * 32, 32), 32)
-        remote(
-            normed_out.at[theirs], normed_out.at[theirs], a_send.at[step], a_recv.at[frm], (sp, frm)
-        ).wait_recv()
-    for step in range(1, 4):
-        to = lax.rem(tp + step, 4)
-        remote(
-            normed_out.at[mine], normed_out.at[mine], a_send.at[step], a_recv.at[tp], (sp, to)
-        ).wait_send()
+        gather(step).wait_send()
+    for who in range(4):
+        pair(who).wait_send()
     for n in range(NC):
         for step in range(1, 4):
             sent(n, step).wait_send()
-
-
-def attend(qn, kn, vn, gn, qb, kb, vb, gb, pn, pb, residual, gain):
+            to_owner(n, step).wait_send()
+        all_of(outb, d_send, n).wait()
+        all_of(back, e_send, n).wait()
+        to_pair(n).wait_send()
+
+
+def layer(*args):
     any_ = pl.BlockSpec(memory_space=pl.ANY)
-    vm = pl.BlockSpec(memory_space=pltpu.VMEM)
     dma = pltpu.SemaphoreType.DMA
     f32, b16 = jnp.float32, jnp.bfloat16
-
-    def rows(g):
-        return (g * LOG2E).T.reshape(g.shape[1], 16, 256).transpose(1, 0, 2)
-
+    vm = pltpu.VMEM
     return pl.pallas_call(
-        attend_kernel,
-        out_shape=(
-            jax.ShapeDtypeStruct((32, 4096), f32),
-            jax.ShapeDtypeStruct((128, 4096), b16),
-        ),
-        in_specs=[any_, any_, any_, vm, any_, any_, any_, vm, any_, any_, any_, vm],
-        out_specs=(vm, vm),
+        layer_kernel,
+        out_shape=jax.ShapeDtypeStruct((32, 4096), b16),
+        in_specs=[any_] * len(args),
+        out_specs=pl.BlockSpec(memory_space=pltpu.VMEM),
         scratch_shapes=[
-            pltpu.VMEM((4, 4, 256, 256), b16),
-            pltpu.VMEM((4, 4, 256, 512), b16),
-            pltpu.VMEM((2, 128, 512), b16),
-            pltpu.VMEM((2, 128, 512), b16),
-            pltpu.VMEM((2, 128, 512), b16),
-            pltpu.VMEM((2, 128, 512), b16),
-            pltpu.VMEM((4, 256, 128), f32),
-            pltpu.VMEM((4, 256, 128), f32),
-            pltpu.VMEM((4, 256, 128), f32),
-            pltpu.VMEM((2, 256, 128), f32),
-            pltpu.VMEM((2, 256, 128), f32),
-            pltpu.VMEM((2, 256, 256), f32),
-            pltpu.VMEM((512, 4096), b16),
-            pltpu.VMEM((512, 4096), b16),
-            pltpu.VMEM((32, 4096), b16),
-            pltpu.VMEM((4, 4, 32, 1024), b16),
-            pltpu.VMEM((4, 4, 32, 1024), b16),
-            dma((3,)), dma((3,)), dma((3,)),
+            vm((4, 4, 256, 256), b16), vm((4, 4, 256, 512), b16),
+            vm((2, 128, 512), b16), vm((2, 128, 512), b16), vm((2, 128, 512), b16), vm((2, 128, 512), b16),
+            vm((4, 256, 128), f32), vm((4, 256, 128), f32), vm((4, 256, 128), f32),
+            vm((2, 256, 128), f32), vm((2, 256, 128), f32), vm((2, 256, 256), f32),
+            vm((512, 4096), b16), vm((512, 4096), b16), vm((32, 4096), b16),
+            vm((4, 4, 32, 1024), b16), vm((4, 4, 32, 1024), b16), vm((32, 4096), f32), vm((2, 128, 4096), b16),
+            vm((4, 4096), f32), vm((2, 4096), f32), vm((1, 4096), f32), vm((4, 32), jnp.int32), vm((4, 32), f32),
+            vm((4096, 512), b16), vm((256, 4096), b16), vm((4096, 512), b16), vm((256, 4096), b16),
+            vm((8, 8, 128), f32), vm((256, 256), b16), vm((2, 128, 256), b16),
+            vm((4, 16, 16, 1024), b16), vm((4, 16, 16, 1024), b16), vm((4, 16, 16, 1024), b16), vm((4, 16, 16, 1024), b16),
+            vm((256, 512), f32), vm((4, 128, 1024), f32),
+            vm((4, 128, 1024), b16), vm((4, 128, 1024), b16), vm((4, 4, 32, 1024), b16), vm((4, 4, 32, 1024), b16),
+            dma((3,)), dma((14,)), dma((3,)),
             dma((4, 2)), dma((4, 2, 2)), dma((4, 2)), dma((4, 2, 2)),
             dma((4, 4)), dma((4, 4)), dma((4, 4)), dma((4, 4)),
             dma((3,)), dma(()), dma(()),
             dma((4, 4)), dma((4, 4)), dma((4,)), dma((4,)),
+            dma((8,)), dma((8,)), dma((4,)), dma((4,)),
+            dma((4,)), dma((4,)), dma((4,)), dma((4,)), dma((4,)), dma((4,)), dma((4, 4)), dma((4, 4)),
         ],
         compiler_params=pltpu.CompilerParams(
-            collective_id=0, has_side_effects=True, vmem_limit_bytes=48 * 2**20
+            collective_id=0, has_side_effects=True, vmem_limit_bytes=67043328
         ),
-        cost_estimate=pl.CostEstimate(flops=4 * 10**9, bytes_accessed=12 * 2**20, transcendentals=3 * 10**6),
-        name="attend",
-    )(qn, kn, vn, rows(gn), qb, kb, vb, rows(gb), pn, pb, residual, gain.reshape(1, -1))
-
-
-def split_up(shard, dim, length):
-    dims = shard.shape
-    parts = shard.reshape(*dims[:dim], length, dims[dim] // length, *dims[dim + 1 :])
-    return jnp.moveaxis(parts, dim, 0)
-
-
-def sum_at_owner(shard, axis, dim):
-    length = lax.axis_size(axis)
-    parts = lax.all_to_all(split_up(shard, dim, length), axis, 0, 0, tiled=True)
-    return jnp.sum(parts.astype(jnp.float32), axis=0)
+        name="layer",
+    )(*args)
 
 
 def local(
-    query_narrow,
-    key_narrow,
-    value_narrow,
-    gates_narrow,
-    query_broad,
-    key_broad,
-    value_broad,
-    gates_broad,
-    project_narrow,
-    project_broad,
-    residual,
-    norm_gain,
-    route_ids,
-    route_weight,
-    expert_gate,
-    expert_up,
-    expert_down,
-    shared_gate,
-    shared_up,
-    shared_down,
+    query_narrow, key_narrow, value_narrow, gates_narrow, query_broad, key_broad, value_broad,
+    gates_broad, project_narrow, project_broad, residual, norm_gain, route_ids, route_weight,
+    expert_gate, expert_up, expert_down, shared_gate, shared_up, shared_down,
 ):
-    own_stream, normed = attend(
-        query_narrow, key_narrow, value_narrow, gates_narrow,
-        query_broad, key_broad, value_broad, gates_broad,
-        project_narrow, project_broad, residual, norm_gain,
+    return layer(
+        query_narrow, key_narrow, value_narrow, gates_narrow.T, query_broad, key_broad, value_broad,
+        gates_broad.T, project_narrow, project_broad, residual, norm_gain.reshape(1, -1), route_ids.T,
+        route_weight.T, expert_gate, expert_up, expert_down, shared_gate, shared_up, shared_down,
     )
-    shared_hidden = (
-        jax.nn.silu(jnp.dot(normed, shared_gate, preferred_element_type=jnp.float32))
-        * jnp.dot(normed, shared_up, preferred_element_type=jnp.float32)
-    ).astype(jnp.bfloat16)
-    sub_rows = route_ids.shape[0]
-    own_first = lax.axis_index("tp") * sub_rows
-    shared = sum_at_owner(
-        jnp.dot(shared_hidden, shared_down, preferred_element_type=jnp.float32).astype(
-            jnp.bfloat16
-        ),
-        "tp",
-        0,
-    )
-    top_count = route_ids.shape[1]
-    local_experts = expert_gate.shape[0]
-    expert_total = lax.axis_size("sp") * lax.axis_size("tp") * local_experts
-    capacity = 2 * sub_rows * top_count // expert_total
-    flat_ids = route_ids.reshape(-1)
-    one_hot = (flat_ids[:, None] == jnp.arange(expert_total, dtype=jnp.int32)[None, :]).astype(
-        jnp.int32
-    )
-    slot_of = jnp.sum(one_hot * (jnp.cumsum(one_hot, axis=0) - 1), axis=1)
-    target = (flat_ids * capacity + slot_of).reshape(sub_rows, top_count)
-    slot_total = expert_total * capacity
-    matches = target[None, :, :] == jnp.arange(slot_total, dtype=jnp.int32)[:, None, None]
-    dispatch = jnp.any(matches, axis=-1).astype(jnp.bfloat16)
-    own_normed = lax.dynamic_slice_in_dim(normed, own_first, sub_rows, 0)
-    outbound = (
-        jnp.dot(dispatch, own_normed, preferred_element_type=jnp.float32)
-        .astype(jnp.bfloat16)
-        .reshape(expert_total, capacity, -1)
-    )
-    weight_rounded = route_weight.astype(jnp.bfloat16)
-    combiner = jnp.sum(
-        jnp.where(matches, weight_rounded[None], jnp.zeros((), jnp.bfloat16)), axis=-1
-    ).T
-    inbound = lax.all_to_all(outbound, ("sp", "tp"), split_axis=0, concat_axis=0, tiled=True)
-    senders = inbound.shape[0] // local_experts
-    grouped = inbound.reshape(senders, local_experts, inbound.shape[1], inbound.shape[2])
-    gate_out = jnp.einsum(
-        "secd,edh->sech", grouped, expert_gate, preferred_element_type=jnp.float32
-    )
-    up_out = jnp.einsum("secd,edh->sech", grouped, expert_up, preferred_element_type=jnp.float32)
-    hidden = (jax.nn.silu(gate_out) * up_out).astype(jnp.bfloat16)
-    result = jnp.einsum(
-        "sech,ehd->secd", hidden, expert_down, preferred_element_type=jnp.float32
-    ).astype(jnp.bfloat16)
-    results = result.reshape(inbound.shape)
-    returned = lax.all_to_all(results, ("sp", "tp"), split_axis=0, concat_axis=0, tiled=True)
-    routed = jnp.dot(combiner, returned.reshape(slot_total, -1), preferred_element_type=jnp.float32)
-    return (own_stream + shared + routed).astype(jnp.bfloat16)
 
 
 def solution(mesh):

time: 187 us -> 135 us (0.72)
  Pallas kernels: 50.7 us -> 133 us
  waiting for transfers between devices: 53.2 us -> 0 us
  starting transfers between devices: 32.1 us -> 0 us
  matrix products: 23.8 us -> 0 us
  local copies, waits for them, and re-layouts: 22.5 us -> 1.67 us
  other arithmetic: 3.91 us -> 0 us
    pallas_call x1, Pallas kernels: 50.7 us -> 133 us  [layer(): pl.pallas_call(layer_kernel, out_shape=jax.ShapeDtypeStruct((32, 4096), b...]
    all_to_all x3 -> x0, waiting for transfers between devices: 53.2 us -> none  [the longest x1 29.3 us: local(): lax.all_to_all(results, ('sp', 'tp'), split_axis=0, concat_axis=0, tiled=...]
    all_to_all x3 -> x0, starting transfers between devices: 32.1 us -> none  [the longest x1 22.4 us: local(): lax.all_to_all(outbound, ('sp', 'tp'), split_axis=0, concat_axis=0, tiled...]
    dot_general x6 -> x0, matrix products: 23.8 us -> none  [the longest x1 7.05 us: local(): jnp.einsum('sech,ehd->secd', hidden, expert_down, preferred_element_type=...]
    reshape x2 -> x0, local copies, waits for them, and re-layouts: 8.47 us -> none  [the longest x1 4.38 us: local(): outbound = jnp.dot(dispatch, own_normed, preferred_element_type=jnp.float...]
    unnamed x27 -> x1, local copies, waits for them, and re-layouts: 8.66 us -> 1.67 us
    convert_element_type x1 -> x0, local copies, waits for them, and re-layouts: 5.13 us -> none  [local(): result = jnp.einsum('sech,ehd->secd', hidden, expert_down, preferred_elem...]
  transfers between devices with their start and end apart: 3 -> 0, of which waited for: 2 -> 0; matrix products, arithmetic and copies ran while one was open for 13% -> 0% of each run, Pallas kernels for 0% -> 0%
where the time goes in v2:
time: 135 us
  Pallas kernels  133 us (99%)
  local copies, waits for them, and re-layouts  1.67 us (1%)
    pallas_call x1, Pallas kernels, layer(): pl.pallas_call(layer_kernel, out_shape=jax.ShapeDtypeStruct((32, 4096), b...  133 us

profile of v2, /device:TPU:1, one launch (start us, length us, event | category | flops | bytes accessed | tf_op | source)
XLA Modules:
  0.0 134.8 jit_solution(11314130565077688600)
XLA Ops:
  0.0 133.1 %layer.1 = bf16[32,4096]{1,0:T(8,128)(2,1)} custom-call(bf16[128,512]{1,0:T(8,128)(2,1)} %qn_in.1, bf16[128,128]{1,0:T(8,128)(2,1)} %kn_in.1, bf16[128,128]{1,0:T(8,128)(2,1)} %vn_in.1, f32[4,4096]{1,0:T(4,128)} %bitcast.5, bf16[128,512]{1,0:T(8,128)(2,1)} %qb_in.1, bf16[128,256]{1,0:T(8,128)(2,1)} %kb_in.1, bf16[128,256]{1,0:T(8,128)(2,1)} %vb_in.1, ...), custom_call_target="tpu_custom_call" | custom-call | tf_op jit(solution)/shard_map/layer/pallas_call | solution.py:540
  133.1 1.7 %copy.22 = bf16[32,4096]{1,0:T(8,128)(2,1)} copy(bf16[32,4096]{1,0:T(8,128)(2,1)} %layer.1) | data formatting | bytes 524288

commit v3 on v2

v3 whole, which is shorter than its diff:
```python
import math

import jax
import jax.numpy as jnp
from jax import lax
from jax.experimental import pallas as pl
from jax.experimental.pallas import tpu as pltpu
from jax.sharding import PartitionSpec as P

norm_epsilon = 1e-06
COLUMNS = 512
BLOCKS = 4096 // COLUMNS
BEHIND = 4
FAR_FIRST = (
    (2, 2), (2, 3), (3, 2), (2, 1), (1, 2), (2, 0), (0, 2), (3, 1), (1, 3), (3, 3), (1, 1), (3, 0), (0, 3),
    (1, 0), (0, 1),
)

MESH = pl.DeviceIdType.MESH
LOG2E = math.log2(math.e)


def flash_heads(q_ref, kv, gate_rows, m_ref, l_ref, acc_ref, heads, size, diagonal):
    keys = kv[:, :size]
    values = kv[:, size:]
    rows = q_ref.shape[0] * q_ref.shape[1]
    length = keys.shape[0]
    scale = size ** (-0.5) * LOG2E
    for h in range(heads):
        q = q_ref[:, :, h * size : (h + 1) * size].reshape(rows, size)
        s = lax.dot_general(q, keys, (((1,), (1,)), ((), ())), preferred_element_type=jnp.float32)
        s = s * scale - gate_rows[h : h + 1, :]
        if diagonal:
            at = lax.broadcasted_iota(jnp.int32, (rows, length), 0)
            to = lax.broadcasted_iota(jnp.int32, (rows, length), 1)
            s = jnp.where(to <= at, s, -jnp.inf)
        top = jnp.broadcast_to(jnp.max(s, axis=1, keepdims=True), (rows, 128))
        if not diagonal:
            before = m_ref[h]
            top = jnp.maximum(before, top)
        p = jnp.exp2(s - jnp.concatenate([top] * (length // 128), axis=1))
        total = jnp.broadcast_to(jnp.sum(p, axis=1, keepdims=True), (rows, 128))
        out = jnp.dot(p.astype(jnp.bfloat16), values, preferred_element_type=jnp.float32)
        if not diagonal:
            factor = jnp.exp2(before - top)
            total = total + l_ref[h] * factor
            out = out + acc_ref[h] * jnp.concatenate([factor] * (size // 128), axis=1)
        m_ref[h] = top
        l_ref[h] = total
        acc_ref[h] = out


def layer_kernel(
    qn_in, kn_in, vn_in, gn_in, qb_in, kb_in, vb_in, gb_in, pn_in, pb_in, res_in, gain_in,
    ids_in, rw_in, eg_in, eu_in, ed_in, sg_in, su_in, sd_in,
    out_ref,
    nkv, bkv, qn, qb, attn, held, mn, ln, accn, mb, lb, accb, wn, wb, res, part, got, stream, normed,
    gn, gb, gain, ids, rw, wgu, wd, sgu, sd, codes, scales, rout, rin, dmat, cmat, outb, inb, back, ret, gu, mine,
    theirs, from_pair, part2, got2, part3, got3,
    own_sem, load_sem, own_send, n1_send, n1_recv, b1_send, b1_recv, n2_send, n2_recv, b2_send,
    b2_recv, q_recv, swap_send, swap_recv, r_send, r_recv, a_send, a_recv,
    c_send, c_recv, p_send, p_recv, d_send, d_recv, e_send, e_recv, t_send, t_recv, s_send, s_recv,
    g_send, g_recv, h_send, h_recv, t3_send, t3_recv,
):
    sp = lax.axis_index("sp")
    tp = lax.axis_index("tp")
    z = sp // 8
    y = (sp // 2) % 4
    c = sp % 2
    half = pl.ds(pl.multiple_of(c * 128, 128), 128)

    def at(zz, yy, cc):
        return (zz * 8 + yy * 2 + cc, tp)

    barrier = pltpu.get_barrier_semaphore()

    def greet(to):
        pl.semaphore_signal(barrier, inc=1, device_id=to, device_id_type=MESH)

    def greet_chip(t, carry):
        greet(at(lax.rem(z + t // 4, 4), lax.rem(y + t % 4, 4), c))
        return carry

    lax.fori_loop(1, 16, greet_chip, 0)
    for step in range(1, 4):
        greet(at(lax.rem(z + step, 4), y, 1 - c))
        greet(at(z, lax.rem(y + step, 4), 1 - c))
        for cc in range(2):
            greet((z * 8 + y * 2 + cc, lax.rem(tp + step, 4)))
    greet(at(z, y, 1 - c))

    loads = [
        (gn_in, gn), (gb_in, gb), (ids_in, ids), (rw_in, rw), (gain_in, gain),
        (res_in.at[pl.ds(pl.multiple_of(tp * 32, 32), 32)], res),
        (pn_in, wn), (pb_in, wb),
        (sg_in, sgu.at[:, pl.ds(0, 256)]), (su_in, sgu.at[:, pl.ds(256, 256)]), (sd_in, sd),
        (eg_in.at[0], wgu.at[:, pl.ds(0, 256)]), (eu_in.at[0], wgu.at[:, pl.ds(256, 256)]),
        (ed_in.at[0], wd),
    ]

    def load(i):
        return pltpu.make_async_copy(loads[i][0], loads[i][1], load_sem.at[i])

    for i in range(6):
        load(i).start()
    pl.semaphore_wait(barrier, 28)

    def remote(src, dst, send, recv, to):
        return pltpu.make_async_remote_copy(
            src_ref=src, dst_ref=dst, send_sem=send, recv_sem=recv, device_id=to, device_id_type=MESH
        )

    own_n = nkv.at[z, y, half]
    own_b = bkv.at[z, y, half]
    owns = (
        (kn_in, nkv.at[z, y, half, pl.ds(0, 128)]), (vn_in, nkv.at[z, y, half, pl.ds(128, 128)]),
        (kb_in, bkv.at[z, y, half, pl.ds(0, 256)]), (vb_in, bkv.at[z, y, half, pl.ds(256, 256)]),
    )

    def own(i):
        return pltpu.make_async_copy(owns[i][0], owns[i][1], own_sem.at[i])

    q_sides = ((qn_in, qn), (qb_in, qb))

    def q_own(role):
        return pltpu.make_async_copy(q_sides[role][0], q_sides[role][1].at[c], own_sem.at[4])

    def q_over(role):
        return remote(
            q_sides[role][0], q_sides[role][1].at[c], own_send.at[0], q_recv.at[0], at(z, y, role)
        )

    def kv_over(role):
        block = (own_n, own_b)[role]
        return remote(block, block, own_send.at[1], q_recv.at[1], at(z, y, role))

    def n1(step):
        return remote(own_n, own_n, n1_send.at[step], n1_recv.at[z, c], at(z + step, y, 0))

    def b1(step):
        return remote(
            own_b, own_b, b1_send.at[step], b1_recv.at[y, c], at(z, lax.rem(y + step, 4), 1)
        )

    for i in range(4):
        own(i).start()
    for role in range(2):

        @pl.when(c == role)
        def _(role=role):
            q_own(role).start()
            q_over(1 - role).start()

    for i in range(4):
        own(i).wait()
    for step in (1, 3, 2):
        b1(step).start()

        @pl.when(z + step < 4)
        def _(step=step):
            n1(step).start()

    for role in range(2):

        @pl.when(c == role)
        def _(role=role):
            kv_over(1 - role).start()

    me = c * 4 + tp
    for i in range(4):
        load(i).wait()
    lane = lax.broadcasted_iota(jnp.int32, (8, 128), 1)
    row = lax.broadcasted_iota(jnp.int32, (32, 128), 0)
    place = lax.broadcasted_iota(jnp.int32, (32, 128), 1) == row + tp * 32
    spot = place.astype(jnp.bfloat16)
    put = lambda a: jnp.dot(a.astype(jnp.bfloat16), spot, preferred_element_type=jnp.float32)
    placed_ids = put(ids[...].astype(jnp.float32))
    placed_rw = put(rw[...])
    inside = (lane[:4] // 32) == tp
    key_ids = jnp.where(inside, placed_ids, -1.0)
    names = lax.broadcasted_iota(jnp.int32, (128, 128), 0).astype(jnp.float32)
    later = (
        lax.broadcasted_iota(jnp.int32, (128, 128), 0) < lax.broadcasted_iota(jnp.int32, (128, 128), 1)
    ).astype(jnp.bfloat16)
    hits = [jnp.where(key_ids[k : k + 1] == names, 1.0, 0.0) for k in range(4)]
    before = jnp.dot(
        (hits[0] + hits[1] + hits[2] + hits[3]).astype(jnp.bfloat16), later,
        preferred_element_type=jnp.float32,
    )
    for k in range(4):
        rank = jnp.sum(hits[k] * before, axis=0, keepdims=True)
        codes[me, k : k + 1] = placed_ids[k : k + 1] * 2.0 + rank
        codes[me, 4 + k : 5 + k] = placed_rw[k : k + 1]

    def code(t):
        to = lax.rem(me + t, 8)
        return remote(
            codes.at[me], codes.at[me], c_send.at[t], c_recv.at[t], (z * 8 + y * 2 + to // 4, to % 4)
        )

    for t in range(1, 8):
        code(t).start()

    def gate_rows(ref, zz, yy):
        return ref[:, pl.ds(pl.multiple_of((zz * 4 + yy) * 256, 256), 256)] * LOG2E

    def own_wait(role):
        block = (nkv, bkv)[role].at[z, y, pl.ds((1 - role) * 128, 128)]
        remote(block, block, own_send.at[1], q_recv.at[1], at(z, y, 1 - role)).wait_recv()

    def q_wait(role):
        q_own(role).wait()
        there = q_sides[role][1].at[1 - c]
        remote(there, there, own_send.at[0], q_recv.at[0], at(z, y, 1 - role)).wait_recv()

    def n2(zz, step):
        return remote(
            nkv.at[zz, y], nkv.at[zz, y], n2_send.at[zz, step], n2_recv.at[zz, y],
            at(z, lax.rem(y + step, 4), 0),
        )

    def b2(yy, step):
        return remote(
            bkv.at[z, yy], bkv.at[z, yy], b2_send.at[yy, step], b2_recv.at[z, yy],
            at(z + step, y, 1),
        )

    @pl.when(c == 0)
    def _():
        own_wait(0)
        q_wait(0)

        def send_on(zz):
            for step in range(1, 4):
                @pl.when((zz < z) | (y + step < 4))
                def _(step=step):
                    n2(zz, step).start()

        def block(zz, yy, diagonal):
            flash_heads(
                qn, nkv[zz, yy], gate_rows(gn, zz, yy), mn, ln, accn, 4, 128, diagonal
            )

        block(z, y, True)
        for step in range(1, 4):
            b1(step).wait_send()
        send_on(z)

        def column(t, carry):
            zz = z - t
            for cc in range(2):
                there = nkv.at[zz, y, pl.ds(cc * 128, 128)]
                remote(there, there, n1_send.at[1], n1_recv.at[zz, cc], at(zz, y, 0)).wait_recv()
            send_on(zz)
            return carry

        lax.fori_loop(1, z + 1, column, 0)
        for i in range(6, 14):
            load(i).start()

        def column_block(t, carry):
            block(z - t, y, False)
            return carry

        lax.fori_loop(1, z + 1, column_block, 0)

        def rest(t, carry):
            zz = z - t // 3
            yy = lax.rem(y + t % 3 + 1, 4)

            @pl.when((zz < z) | (yy < y))
            def _():
                remote(
                    nkv.at[zz, yy], nkv.at[zz, yy], n2_send.at[zz, 1], n2_recv.at[zz, yy],
                    at(z, yy, 0),
                ).wait_recv()
                block(zz, yy, False)

            return carry

        lax.fori_loop(0, 3 * (z + 1), rest, 0)
        for h in range(4):
            out = (accn[h] / ln[h]).astype(jnp.bfloat16)
            held[:, :, h * 128 : (h + 1) * 128] = out.reshape(2, 128, 128)
        remote(
            held.at[1], attn.at[0], swap_send, swap_recv, at(z, y, 1)
        ).start()
        attn[0] = held[0]

    @pl.when(c == 1)
    def _():
        own_wait(1)

        def send_on(yy):
            for step in range(1, 4):
                @pl.when(z + step < 4)
                def _(step=step):
                    b2(yy, step).start()

        def block(zz, yy, diagonal):
            flash_heads(qb, bkv[zz, yy], gate_rows(gb, zz, yy), mb, lb, accb, 2, 256, diagonal)

        send_on(y)
        q_wait(1)
        block(z, y, True)

        def turn(t):
            return lax.rem(y + jnp.where(t == 2, 3, jnp.where(t == 3, 2, t)), 4)

        def row(t, carry):
            yy = turn(t)
            for cc in range(2):
                there = bkv.at[z, yy, pl.ds(cc * 128, 128)]
                remote(there, there, b1_send.at[1], b1_recv.at[yy, cc], at(z, yy, 1)).wait_recv()
            send_on(yy)
            return carry

        lax.fori_loop(1, 4, row, 0)
        for i in range(6, 14):
            load(i).start()

        def row_block(t, carry):
            block(z, t, False)
            return carry

        lax.fori_loop(0, y, row_block, 0)

        def rest(t, carry):
            yy = turn(t)

            def one(k, inner):
                zz = z - k
                remote(
                    bkv.at[zz, yy], bkv.at[zz, yy], b2_send.at[yy, 1], b2_recv.at[zz, yy],
                    at(zz, y, 1),
                ).wait_recv()
                block(zz, yy, False)
                return inner

            return lax.fori_loop(1, z + 1, one, carry)

        lax.fori_loop(0, 4, rest, 0)
        for h in range(2):
            out = (accb[h] / jnp.concatenate([lb[h]] * 2, axis=1)).astype(jnp.bfloat16)
            held[:, :, h * 256 : (h + 1) * 256] = out.reshape(2, 128, 256)
        remote(
            held.at[0], attn.at[1], swap_send, swap_recv, at(z, y, 0)
        ).start()
        attn[1] = held[1]

    remote(held.at[1 - c], attn.at[1 - c], swap_send, swap_recv, at(z, y, 1 - c)).wait_recv()
    for i in range(4, 8):
        load(i).wait()

    CH = COLUMNS
    NC = 4096 // CH
    chip = z * 4 + y
    rows_of = lambda who: pl.ds(pl.multiple_of(who * 32, 32), 32)

    def sent(n, step):
        to = lax.rem(tp + step, 4)
        return remote(
            part.at[n, to], got.at[n, step], r_send.at[n, step], r_recv.at[n, step], (sp, to)
        )

    def gather(n, step):
        to = lax.rem(tp + step, 4)
        block = normed.at[n, c, rows_of(tp)]
        return remote(block, block, a_send.at[n, step], a_recv.at[n, step], (sp, to))

    def arrived(n, step):
        frm = lax.rem(tp + 4 - step, 4)
        block = normed.at[n, c, rows_of(frm)]
        return remote(block, block, a_send.at[n, step], a_recv.at[n, step], (sp, frm))

    def pair(n, step):
        block = normed.at[n, c, rows_of(lax.rem(tp + 4 - step, 4))]
        return remote(block, block, p_send.at[n, step], p_recv.at[n, step], at(z, y, 1 - c))

    def slots(src, dst, send, recv, n):
        for dz, dy in FAR_FIRST:
            zz = lax.rem(z + jnp.where(c == 0, dz, 4 - dz), 4)
            yy = lax.rem(y + jnp.where(c == 0, dy, 4 - dy), 4)
            remote(
                src.at[n, zz * 4 + yy], dst.at[n, chip], send.at[n], recv.at[n], at(zz, yy, c)
            ).start()

    def all_of(ref, sem, n):
        block = ref.at[n, pl.ds(0, 15)]
        return pltpu.make_async_copy(block, block, sem.at[n])

    for t in range(1, 8):
        code(t).wait_recv()

    def chip_line(ref):
        return jnp.concatenate(
            [ref[h * 4] + ref[h * 4 + 1] + ref[h * 4 + 2] + ref[h * 4 + 3] for h in range(2)], axis=1
        )

    table = chip_line(codes)
    slot = lax.broadcasted_iota(jnp.int32, (256, 256), 0)
    token = lax.broadcasted_iota(jnp.int32, (256, 256), 1)
    wanted = (((slot // 16) * 2 + c) * 4 + tp) * 2 + slot % 2
    wanted = jnp.where((slot // 2) % 8 == token // 32, wanted, -1).astype(jnp.float32)
    picks = jnp.zeros((256, 256), jnp.float32)
    pays = jnp.zeros((256, 256), jnp.float32)
    for k in range(4):
        same = table[k : k + 1] == wanted
        picks = picks + jnp.where(same, 1.0, 0.0)
        pays = pays + jnp.where(same, table[4 + k : 5 + k], 0.0)
    dmat[...] = picks.astype(jnp.bfloat16)
    cmat[...] = pays.T.reshape(2, 128, 256).astype(jnp.bfloat16)

    def project(n):
        cols = pl.ds(n * CH, CH)
        p = jnp.dot(attn[0], wn[:, cols], preferred_element_type=jnp.float32)
        p = p + jnp.dot(attn[1], wb[:, cols], preferred_element_type=jnp.float32)
        part[n] = p.astype(jnp.bfloat16).reshape(4, 32, CH)
        for step in range(1, 4):
            sent(n, step).start()

    squares = []

    def add_up(n):
        for step in range(1, 4):
            sent(n, step).wait_recv()
        cols = pl.ds(n * CH, CH)
        total = res[:, cols].astype(jnp.float32) + part[n, tp].astype(jnp.float32)
        for step in range(1, 4):
            total = total + got[n, step].astype(jnp.float32)
        stream[:, cols] = total
        normed[n, c, rows_of(tp)] = (total * gain[:, cols]).astype(jnp.bfloat16)
        for step in range(1, 4):
            gather(n, step).start()
        pair(n, 0).start()
        sq = total * total
        for k in range(CH // 128):
            squares.append(sq[:, k * 128 : (k + 1) * 128])

    def forward(n):
        for step in range(1, 4):
            arrived(n, step).wait_recv()
            pair(n, step).start()

    def paired(n, step):
        block = normed.at[n, 1 - c, rows_of(lax.rem(tp + 4 - step, 4))]
        return remote(block, block, p_send.at[n, step], p_recv.at[n, step], at(z, y, 1 - c))

    def dispatch(n):
        for step in range(4):
            paired(n, step).wait_recv()
        rows = normed[n].reshape(256, CH)
        picked = jnp.dot(dmat[...], rows, preferred_element_type=jnp.float32).astype(jnp.bfloat16)
        outb[n] = picked.reshape(16, 16, CH)
        slots(outb, inb, d_send, d_recv, n)
        inb[n, chip] = outb[n, chip]

    def rate(t):
        to = lax.rem(me + t, 8)
        return remote(
            scales.at[me], scales.at[me], g_send.at[t], g_recv.at[t], (z * 8 + y * 2 + to // 4, to % 4)
        )

    def take_in(n):
        all_of(inb, d_recv, n).wait()
        more = jnp.dot(
            inb[n].reshape(256, CH), wgu[n * CH : (n + 1) * CH, :], preferred_element_type=jnp.float32
        )
        gu[...] = more if n == 0 else gu[...] + more

    for i in range(8, 14):
        load(i).wait()
    project(0)
    project(1)
    for i in range(NC + 2):
        if i < NC:
            add_up(i)
        if i == NC - 1:
            mean = jnp.sum(sum(squares[1:], squares[0]), axis=1, keepdims=True) * (1.0 / 4096)
            own_rate = lax.rsqrt(mean + norm_epsilon)
            scales[me] = jnp.broadcast_to(
                jnp.sum(jnp.where(place, own_rate, 0.0), axis=0, keepdims=True), (8, 128)
            )
            for t in range(1, 8):
                rate(t).start()
        if i + 2 < NC:
            project(i + 2)
        if 0 <= i - 1 < NC:
            forward(i - 1)
        if i - 2 == NC - 1:
            for t in range(1, 8):
                rate(t).wait_recv()
            rates = chip_line(scales)[:1]
            by_slot = jnp.sum(picks * rates, axis=1, keepdims=True)
            high = by_slot.astype(jnp.bfloat16).astype(jnp.float32)
            first = lax.broadcasted_iota(jnp.int32, (256, 128), 1)
            pieces = jnp.where(first == 0, high, jnp.where(first == 1, by_slot - high, 0.0))
            rout[0] = pieces.astype(jnp.bfloat16).reshape(16, 16, 128)
            slots(rout, rin, h_send, h_recv, 0)
            rin[0, chip] = rout[0, chip]
        if 0 <= i - 2:
            dispatch(i - 2)
        if 0 <= i - 1 - BEHIND:
            take_in(i - 1 - BEHIND)

    for n in range(NC + 1 - BEHIND, NC):
        take_in(n)
    def silu_up(both):
        gate, up = both[:, :256], both[:, 256:]
        return (gate / (1.0 + jnp.exp(-gate)) * up).astype(jnp.bfloat16)

    all_of(rin, h_recv, 0).wait()
    hidden = silu_up(
        gu[...] * jnp.sum(rin[0].reshape(256, 128).astype(jnp.float32), axis=1, keepdims=True)
    )
    for n in range(NC):
        made = jnp.dot(hidden, wd[:, n * CH : (n + 1) * CH], preferred_element_type=jnp.float32)
        back[n] = made.astype(jnp.bfloat16).reshape(16, 16, CH)
        slots(back, ret, e_send, e_recv, n)
        ret[n, chip] = back[n, chip]

    lanes = lax.broadcasted_iota(jnp.int32, (128, 256), 1)
    mark_row = lanes == lax.broadcasted_iota(jnp.int32, (128, 256), 0) + c * 128
    by_token = jnp.sum(jnp.where(mark_row, rates, 0.0), axis=1, keepdims=True)

    both = jnp.dot(normed[0, c], sgu[:CH, :], preferred_element_type=jnp.float32)
    for n in range(1, NC):
        both = both + jnp.dot(
            normed[n, c], sgu[n * CH : (n + 1) * CH, :], preferred_element_type=jnp.float32
        )
    hidden = silu_up(both * by_token)
    for n in range(NC):
        mine[n] = jnp.dot(hidden, sd[:, n * CH : (n + 1) * CH], preferred_element_type=jnp.float32)

    def to_pair(n):
        return remote(theirs.at[n], from_pair.at[n], t_send.at[n], t_recv.at[n], at(z, y, 1 - c))

    def to_owner(n, step):
        to = lax.rem(tp + step, 4)
        return remote(
            part2.at[n, to], got2.at[n, step], s_send.at[n, step], s_recv.at[n, step], (sp, to)
        )

    def over(step):
        to = lax.rem(tp + step, 4)
        return remote(
            part3.at[to], got3.at[step], t3_send.at[step], t3_recv.at[step],
            (z * 8 + y * 2 + 1 - c, to),
        )

    last = NC - 1

    def finish(n):
        total = stream[:, n * CH : (n + 1) * CH] + part2[n, tp].astype(jnp.float32)
        for step in range(1, 4):
            to_owner(n, step).wait_recv()
            total = total + got2[n, step].astype(jnp.float32)
        if n == last:
            for step in range(4):
                over(step).wait_recv()
                total = total + got3[step].astype(jnp.float32)
        out_ref[:, n * CH : (n + 1) * CH] = total

    def merge(n):
        to_pair(n).wait_recv()
        both = mine[n] + from_pair[n].astype(jnp.float32)
        part2[n] = both.astype(jnp.bfloat16).reshape(4, 32, CH)
        for step in range(1, 4):
            to_owner(n, step).start()

    for i in range(NC):
        all_of(ret, e_recv, i).wait()
        rows = ret[i].reshape(256, CH)
        away = jnp.dot(cmat[1 - c], rows, preferred_element_type=jnp.float32).astype(jnp.bfloat16)
        if i < last:
            theirs[i] = away
            to_pair(i).start()
            mine[i] = mine[i] + jnp.dot(cmat[c], rows, preferred_element_type=jnp.float32)
        else:
            part3[...] = away.reshape(4, 32, CH)
            for step in (2, 1, 3, 0):
                over(step).start()
            ours = mine[i] + jnp.dot(cmat[c], rows, preferred_element_type=jnp.float32)
            part2[i] = ours.astype(jnp.bfloat16).reshape(4, 32, CH)
            for step in (2, 1, 3):
                to_owner(i, step).start()
        if 0 <= i - 1:
            merge(i - 1)
        if 0 <= i - 2:
            finish(i - 2)
    finish(last - 1)
    finish(last)

    for role in range(2):

        @pl.when(c == role)
        def _(role=role):
            q_over(1 - role).wait_send()
            kv_over(1 - role).wait_send()

    for step in range(1, 4):

        @pl.when(c == 1)
        def _(step=step):
            b1(step).wait_send()

        @pl.when(z + step < 4)
        def _(step=step):
            n1(step).wait_send()

    @pl.when(c == 0)
    def _():
        def done(t, carry):
            for step in range(1, 4):

                @pl.when((t < z) | (y + step < 4))
                def _(step=step):
                    n2(t, step).wait_send()

            return carry

        lax.fori_loop(0, z + 1, done, 0)

    @pl.when(c == 1)
    def _():
        def done(t, carry):
            for step in range(1, 4):

                @pl.when(z + step < 4)
                def _(step=step):
                    b2(t, step).wait_send()

            return carry

        lax.fori_loop(0, 4, done, 0)

    remote(held.at[1 - c], attn.at[1 - c], swap_send, swap_recv, at(z, y, 1 - c)).wait_send()
    for t in range(1, 8):
        code(t).wait_send()
    for step in range(4):
        over(step).wait_send()
    for t in range(1, 8):
        rate(t).wait_send()
    all_of(rout, h_send, 0).wait()
    for n in range(NC):
        for step in range(1, 4):
            gather(n, step).wait_send()
        for step in range(4):
            pair(n, step).wait_send()
        for step in range(1, 4):
            sent(n, step).wait_send()
            to_owner(n, step).wait_send()
        all_of(outb, d_send, n).wait()
        all_of(back, e_send, n).wait()
        if n < last:
            to_pair(n).wait_send()


def layer(*args):
    any_ = pl.BlockSpec(memory_space=pltpu.HBM)
    dma = pltpu.SemaphoreType.DMA
    f32, b16 = jnp.float32, jnp.bfloat16
    vm = pltpu.VMEM
    return pl.pallas_call(
        layer_kernel,
        out_shape=jax.ShapeDtypeStruct((32, 4096), f32),
        in_specs=[any_] * len(args),
        out_specs=pl.BlockSpec(memory_space=pltpu.VMEM),
        scratch_shapes=[
            vm((4, 4, 256, 256), b16), vm((4, 4, 256, 512), b16),
            vm((2, 128, 512), b16), vm((2, 128, 512), b16), vm((2, 128, 512), b16), vm((2, 128, 512), b16),
            vm((4, 256, 128), f32), vm((4, 256, 128), f32), vm((4, 256, 128), f32),
            vm((2, 256, 128), f32), vm((2, 256, 128), f32), vm((2, 256, 256), f32),
            vm((512, 4096), b16), vm((512, 4096), b16), vm((32, 4096), b16),
            vm((BLOCKS, 4, 32, COLUMNS), b16), vm((BLOCKS, 4, 32, COLUMNS), b16), vm((32, 4096), f32),
            vm((BLOCKS, 2, 128, COLUMNS), b16),
            vm((4, 4096), f32), vm((2, 4096), f32), vm((1, 4096), f32), vm((4, 32), jnp.int32), vm((4, 32), f32),
            vm((4096, 512), b16), vm((256, 4096), b16), vm((4096, 512), b16), vm((256, 4096), b16),
            vm((8, 8, 128), f32), vm((8, 8, 128), f32), vm((1, 16, 16, 128), b16), vm((1, 16, 16, 128), b16),
            vm((256, 256), b16), vm((2, 128, 256), b16),
            *[vm((BLOCKS, 16, 16, COLUMNS), b16)] * 4,
            vm((256, 512), f32), vm((BLOCKS, 128, COLUMNS), f32),
            vm((BLOCKS, 128, COLUMNS), b16), vm((BLOCKS, 128, COLUMNS), b16),
            vm((BLOCKS, 4, 32, COLUMNS), b16), vm((BLOCKS, 4, 32, COLUMNS), b16),
            vm((4, 32, COLUMNS), b16), vm((4, 32, COLUMNS), b16),
            dma((5,)), dma((14,)), dma((2,)),
            dma((4,)), dma((4, 2)), dma((4,)), dma((4, 2)),
            dma((4, 4)), dma((4, 4)), dma((4, 4)), dma((4, 4)),
            dma((2,)), dma(()), dma(()),
            dma((BLOCKS, 4)), dma((BLOCKS, 4)), dma((BLOCKS, 4)), dma((BLOCKS, 4)),
            dma((8,)), dma((8,)), dma((BLOCKS, 4)), dma((BLOCKS, 4)),
            dma((BLOCKS,)), dma((BLOCKS,)), dma((BLOCKS,)), dma((BLOCKS,)), dma((BLOCKS,)), dma((BLOCKS,)),
            dma((BLOCKS, 4)), dma((BLOCKS, 4)),
            dma((8,)), dma((8,)), dma((1,)), dma((1,)), dma((4,)), dma((4,)),
        ],
        compiler_params=pltpu.CompilerParams(
            collective_id=0, has_side_effects=True, vmem_limit_bytes=56 * 2**20
        ),
        name="layer",
    )(*args)


def local(
    query_narrow, key_narrow, value_narrow, gates_narrow, query_broad, key_broad, value_broad,
    gates_broad, project_narrow, project_broad, residual, norm_gain, route_ids, route_weight,
    expert_gate, expert_up, expert_down, shared_gate, shared_up, shared_down,
):
    return layer(
        query_narrow, key_narrow, value_narrow, gates_narrow.T, query_broad, key_broad, value_broad,
        gates_broad.T, project_narrow, project_broad, residual, norm_gain.reshape(1, -1), route_ids.T,
        route_weight.T, expert_gate, expert_up, expert_down, shared_gate, shared_up, shared_down,
    ).astype(jnp.bfloat16)


def solution(mesh):
    placed = (
        P("sp", "tp"),
        P("sp", "tp"),
        P("sp", "tp"),
        P(None, "tp"),
        P("sp", "tp"),
        P("sp", "tp"),
        P("sp", "tp"),
        P(None, "tp"),
        P("tp", None),
        P("tp", None),
        P("sp", None),
        P(),
        P(("sp", "tp"), None),
        P(("sp", "tp"), None),
        P(("sp", "tp"), None, None),
        P(("sp", "tp"), None, None),
        P(("sp", "tp"), None, None),
        P(None, "tp"),
        P(None, "tp"),
        P("tp", None),
    )
    return jax.shard_map(
        local, mesh=mesh, in_specs=placed, out_specs=P(("sp", "tp"), None), check_vma=False
    )
```

time: 135 us -> 115 us (0.85)
  Pallas kernels: 133 us -> 112 us
  other arithmetic: 0 us -> 1.77 us
  local copies, waits for them, and re-layouts: 1.67 us -> 0 us
    pallas_call x1, Pallas kernels: 133 us -> 112 us  [layer(): pl.pallas_call(layer_kernel, out_shape=jax.ShapeDtypeStruct((32, 4096), f...]
    convert_element_type x0 -> x1, other arithmetic: none -> 1.77 us  [local(): return layer(query_narrow, key_narrow, value_narrow, gates_narrow.T, quer...]
    unnamed x1 -> x0, local copies, waits for them, and re-layouts: 1.67 us -> none
where the time goes in v3:
time: 115 us; the launch traced here: 114 us
  Pallas kernels  112 us (97%)
  other arithmetic  1.77 us (2%)
    pallas_call x1, Pallas kernels, layer(): pl.pallas_call(layer_kernel, out_shape=jax.ShapeDtypeStruct((32, 4096), f...  112 us

profile of v3, /device:TPU:1, one launch (start us, length us, event | category | flops | bytes accessed | tf_op | source)
XLA Modules:
  0.0 114.0 jit_solution(11781565905229595011)
XLA Ops:
  0.0 112.3 %layer.1 = f32[32,4096]{1,0:T(8,128)} custom-call(bf16[128,512]{1,0:T(8,128)(2,1)} %qn_in.1, bf16[128,128]{1,0:T(8,128)(2,1)} %kn_in.1, bf16[128,128]{1,0:T(8,128)(2,1)} %vn_in.1, f32[4,4096]{1,0:T(4,128)} %bitcast.5, bf16[128,512]{1,0:T(8,128)(2,1)} %qb_in.1, bf16[128,256]{1,0:T(8,128)(2,1)} %kb_in.1, bf16[128,256]{1,0:T(8,128)(2,1)} %vb_in.1, ...), custom_call_target="tpu_custom_call" | custom-call | tf_op jit(solution)/shard_map/layer/pallas_call | solution.py:664
  112.3 1.8 %convert_element_type.3 = bf16[32,4096]{1,0:T(8,128)(2,1)} convert(f32[32,4096]{1,0:T(8,128)} %layer.1) | non-fusion elementwise | flops 131072 | bytes 786432 | tf_op jit(solution)/shard_map/convert_element_type | solution.py:712

commit v4 on v3

--- a/solution.py
+++ b/solution.py
@@ -10,10 +10,10 @@
 norm_epsilon = 1e-06
 COLUMNS = 512
 BLOCKS = 4096 // COLUMNS
-BEHIND = 4
+BEHIND = 6
 FAR_FIRST = (
-    (2, 2), (2, 3), (3, 2), (2, 1), (1, 2), (2, 0), (0, 2), (3, 1), (1, 3), (3, 3), (1, 1), (3, 0), (0, 3),
-    (1, 0), (0, 1),
+    (2, 2), (1, 2), (2, 3), (3, 2), (2, 1), (1, 1), (1, 3), (3, 3), (3, 1),
+    (2, 0), (0, 2), (1, 0), (0, 1), (3, 0), (0, 3),
 )
 
 MESH = pl.DeviceIdType.MESH
@@ -153,12 +153,12 @@
 
     for i in range(4):
         own(i).wait()
-    for step in (1, 3, 2):
+    for step, onward in ((1, 3), (3, 2), (2, 1)):
         b1(step).start()
 
-        @pl.when(z + step < 4)
-        def _(step=step):
-            n1(step).start()
+        @pl.when(z + onward < 4)
+        def _(onward=onward):
+            n1(onward).start()
 
     for role in range(2):
 
@@ -292,7 +292,7 @@
         own_wait(1)
 
         def send_on(yy):
-            for step in range(1, 4):
+            for step in (3, 2, 1):
                 @pl.when(z + step < 4)
                 def _(step=step):
                     b2(yy, step).start()

time: 115 us -> 115 us (level)
  no operation moved by 1% of the time
where the time goes in v4:
time: 115 us; the launch traced here: 113 us
  Pallas kernels  112 us (97%)
  other arithmetic  1.77 us (2%)
    pallas_call x1, Pallas kernels, layer(): pl.pallas_call(layer_kernel, out_shape=jax.ShapeDtypeStruct((32, 4096), f...  112 us

profile of v4, /device:TPU:1, one launch (start us, length us, event | category | flops | bytes accessed | tf_op | source)
XLA Modules:
  0.0 113.5 jit_solution(9835059059827803135)
XLA Ops:
  0.0 111.7 %layer.1 = f32[32,4096]{1,0:T(8,128)} custom-call(bf16[128,512]{1,0:T(8,128)(2,1)} %qn_in.1, bf16[128,128]{1,0:T(8,128)(2,1)} %kn_in.1, bf16[128,128]{1,0:T(8,128)(2,1)} %vn_in.1, f32[4,4096]{1,0:T(4,128)} %bitcast.5, bf16[128,512]{1,0:T(8,128)(2,1)} %qb_in.1, bf16[128,256]{1,0:T(8,128)(2,1)} %kb_in.1, bf16[128,256]{1,0:T(8,128)(2,1)} %vb_in.1, ...), custom_call_target="tpu_custom_call" | custom-call | tf_op jit(solution)/shard_map/layer/pallas_call | solution.py:664
  111.7 1.8 %convert_element_type.3 = bf16[32,4096]{1,0:T(8,128)(2,1)} convert(f32[32,4096]{1,0:T(8,128)} %layer.1) | non-fusion elementwise | flops 131072 | bytes 786432 | tf_op jit(solution)/shard_map/convert_element_type | solution.py:712
